TPU v7x, 32 devices: a whole 2x2x4 slice. The times are simulated.
32 devices in a mesh: dp: 4 (over y, x), kv: 4 (over z), tp: 2 (over core).
Axes of the slice: x: 2, y: 2, z: 4, core: 2. Of those that a mesh axis runs over, the one named last changes fastest.
Arguments:
- tokens: bfloat16 [256, 4096], P('dp', 'kv'), may hold values from -24 to 24
- state: float32 [256, 64, 64, 64], P(('dp', 'kv'), 'tp'), may hold values from -4 to 4
- w_query: bfloat16 [4096, 4096], P('kv', 'tp'), may hold values from -0.09375 to 0.09375
- w_forget: bfloat16 [4096, 4096], P('kv', 'tp'), may hold values from -0.09375 to 0.09375
- w_input: bfloat16 [4096, 4096], P('kv', 'tp'), may hold values from -0.09375 to 0.09375
- w_gate: bfloat16 [4096, 4096], P('kv', 'tp'), may hold values from -0.09375 to 0.09375
- lower_bound: float32 [4096], P('tp'), may hold values from 0 to 0.9
- head_gain: float32 [64], replicated, may hold values from 0.1 to 1.9
- w_out: bfloat16 [4096, 4096], P('tp', 'kv'), may hold values from -0.09375 to 0.09375
- gain_one: float32 [4096], P(('kv', 'tp')), may hold values from 0.1 to 1.9
- bias_one: float32 [4096], P(('kv', 'tp')), may hold values from -2 to 2
- w_up: bfloat16 [4096, 16384], P(None, ('kv', 'tp')), may hold values from -0.09375 to 0.09375
- w_down: bfloat16 [16384, 4096], P(('kv', 'tp')), may hold values from -0.0625 to 0.0625
- gain_two: float32 [4096], P(('kv', 'tp')), may hold values from 0.1 to 1.9
- bias_two: float32 [4096], P(('kv', 'tp')), may hold values from -2 to 2
Outputs:
- result: bfloat16 [256, 4096], P('dp', ('kv', 'tp'))
- new_state: float32 [256, 64, 64, 64], P(('dp', 'kv'), 'tp')
All inputs are finite; a program needn't handle non-finite values.
Results may differ from a plain program's by a relative error of at most 0.014.
Values may be sent and summed in bfloat16 or wider, within the bound.
A program may use at most 128 MiB of HBM per device.

v0:
```python
import functools

import jax
import jax.numpy as jnp
import numpy as np
from jax import lax
from jax.experimental import pallas as pl
from jax.experimental.pallas import tpu as pltpu
from jax.sharding import PartitionSpec as P

epsilon = 0.1
residual_scale = 1.68
MESH = pl.DeviceIdType.MESH
VMEM_BYTES = 60 * 1024 * 1024


def shifted(index, by, count):
    return lax.rem(index + by, count)


def greet(peers):
    barrier = pltpu.get_barrier_semaphore()
    for peer in peers:
        pl.semaphore_signal(barrier, inc=1, device_id=peer, device_id_type=MESH)
    return lambda: pl.semaphore_wait(barrier, len(peers))


def send(source, target, send_sem, recv_sem, peer):
    copy = pltpu.make_async_remote_copy(
        src_ref=source,
        dst_ref=target,
        send_sem=send_sem,
        recv_sem=recv_sem,
        device_id=peer,
        device_id_type=MESH,
    )
    copy.start()
    return copy


def project_kernel(
    n,
    chunk,
    size,
    tokens,
    bound,
    wq,
    wf,
    wi,
    wg,
    columns,
    lines,
    wbuf,
    whole,
    sent,
    got,
    load_sem,
    send_sem,
    recv_sem,
):
    me = lax.axis_index("kv")
    weights = (wq, wf, wi, wg)
    per = wq.shape[1] // chunk
    chunks = len(weights) * per
    rows = lines.shape[1]
    peers = [{"kv": shifted(me, o, n)} for o in range(1, n)]
    wait_barrier = greet(peers)
    order = [w * per + j for j in range(per) for w in range(len(weights))]
    loads = {}
    for c in order:
        loads[c] = pltpu.make_async_copy(
            weights[c // per].at[:, pl.ds((c % per) * chunk, chunk)], wbuf.at[c], load_sem.at[c]
        )
        loads[c].start()
    copies = {}
    for c in order:
        loads[c].wait()
        value = jnp.dot(tokens[...], wbuf[c], preferred_element_type=jnp.float32)
        value = value.reshape(n, rows, chunk)
        whole[c] = value
        sent[c] = value.astype(jnp.bfloat16)
        if c == order[0]:
            wait_barrier()
        for o in range(1, n):
            copies[c, o] = send(
                sent.at[c, shifted(me, o, n)],
                got.at[c, o - 1],
                send_sem.at[c, o - 1],
                recv_sem.at[c, o - 1],
                peers[o - 1],
            )

    def summed(c):
        total = whole[c, me]
        for o in range(1, n):
            copies[c, o].wait_recv()
            total = total + got[c, o - 1].astype(jnp.float32)
        return total.astype(jnp.bfloat16).astype(jnp.float32)

    heads = chunk // size
    for j in range(per):
        here = slice(j * chunk, (j + 1) * chunk)
        query_raw, forget_raw, value, gate = (summed(w * per + j) for w in range(len(weights)))
        low = bound[:, here]
        forget = low + (1.0 - low) * jax.nn.sigmoid(forget_raw)
        keyvec = (1.0 - low) * jax.nn.sigmoid(-forget_raw)
        query = query_raw * jax.nn.sigmoid(query_raw)
        for i, factor in enumerate((forget, keyvec, query)):
            high = factor.astype(jnp.bfloat16).astype(jnp.float32)
            stacked = jnp.concatenate([high, factor - high], axis=0)
            turned = stacked.T.reshape(heads, size, 2 * rows).astype(jnp.bfloat16)
            columns[i, j * heads : (j + 1) * heads] = turned
        lines[0, :, here] = value
        lines[1, :, here] = gate * jax.nn.sigmoid(gate)
    for copy in copies.values():
        copy.wait_send()


def project(tokens, bound, weights, n, size):
    count = tokens.shape[0]
    rows = count // n
    depth, width = weights[0].shape
    chunk = min(width, 1024)
    chunks = len(weights) * (width // chunk)
    vmem = pl.BlockSpec(memory_space=pltpu.VMEM)
    return pl.pallas_call(
        functools.partial(project_kernel, n, chunk, size),
        out_shape=(
            jax.ShapeDtypeStruct((3, width // size, size, 2 * rows), jnp.bfloat16),
            jax.ShapeDtypeStruct((2, rows, width), jnp.float32),
        ),
        in_specs=[vmem] * 2 + [pl.BlockSpec(memory_space=pl.ANY)] * len(weights),
        out_specs=(vmem, vmem),
        scratch_shapes=[
            pltpu.VMEM((chunks, depth, chunk), jnp.bfloat16),
            pltpu.VMEM((chunks, n, rows, chunk), jnp.float32),
            pltpu.VMEM((chunks, n, rows, chunk), jnp.bfloat16),
            pltpu.VMEM((chunks, n - 1, rows, chunk), jnp.bfloat16),
            pltpu.SemaphoreType.DMA((chunks,)),
            pltpu.SemaphoreType.DMA((chunks, n - 1)),
            pltpu.SemaphoreType.DMA((chunks, n - 1)),
        ],
        compiler_params=pltpu.CompilerParams(
            collective_id=0, has_side_effects=True, vmem_limit_bytes=VMEM_BYTES
        ),
        name="project",
    )(tokens, bound, *weights)


def state_kernel(state, columns, lines, gain, pick, new_state, mixout, spread, value, read):
    count, heads, size, _ = state.shape
    lanes = pick.shape[1] // count
    factors = columns[...].reshape(3 * heads * size, 2 * count)
    spread[...] = jnp.dot(factors, pick[...], preferred_element_type=jnp.float32)

    def turned(values, h):
        return pltpu.roll(values, (heads - h) * size, 1) if h else values

    for h in range(heads):
        value[h] = turned(lines[0], h)
    gated = []
    for h in range(heads):
        for b in range(count):
            forget, keyvec, query = (
                spread[
                    (i * heads + h) * size : (i * heads + h + 1) * size,
                    b * lanes : b * lanes + size,
                ]
                for i in range(3)
            )
            updated = forget * state[b, h] + keyvec * value[h, b : b + 1, :size]
            new_state[b, h] = updated
            read[h, b : b + 1] = jnp.sum(updated * query, axis=0, keepdims=True)
    for h in range(heads):
        whole = read[h]
        scale = lax.rsqrt(jnp.mean(whole * whole, axis=1, keepdims=True) + epsilon)
        gated.append(whole * scale * gain[...] * turned(lines[1], h)[:, :size])
    mixout[...] = jnp.concatenate(gated, axis=1).astype(jnp.bfloat16)


def update_state(state, columns, lines, gain):
    count, heads, size, _ = state.shape
    lanes = 128
    some = lanes // size
    pick = np.arange(2 * count)[:, None] % count == np.arange(count * lanes) // lanes
    pick = jnp.asarray(pick, jnp.bfloat16)
    return pl.pallas_call(
        state_kernel,
        grid=(heads // some,),
        out_shape=(
            jax.ShapeDtypeStruct(state.shape, jnp.float32),
            jax.ShapeDtypeStruct((count, heads * size), jnp.bfloat16),
        ),
        in_specs=[
            pl.BlockSpec((count, some, size, size), lambda h: (0, h, 0, 0)),
            pl.BlockSpec((3, some, size, 2 * count), lambda h: (0, h, 0, 0)),
            pl.BlockSpec((2, count, lanes), lambda h: (0, 0, h)),
            pl.BlockSpec((1, size), lambda h: (0, 0)),
            pl.BlockSpec((2 * count, count * lanes), lambda h: (0, 0)),
        ],
        out_specs=(
            pl.BlockSpec((count, some, size, size), lambda h: (0, h, 0, 0)),
            pl.BlockSpec((count, lanes), lambda h: (0, h)),
        ),
        scratch_shapes=[
            pltpu.VMEM((3 * some * size, count * lanes), jnp.float32),
            pltpu.VMEM((some, count, lanes), jnp.float32),
            pltpu.VMEM((some, count, size), jnp.float32),
        ],
        compiler_params=pltpu.CompilerParams(vmem_limit_bytes=VMEM_BYTES),
        name="state",
    )(state, columns, lines, gain, pick)


def to_lanes(column):
    count = column.shape[0]
    diagonal = lax.broadcasted_iota(jnp.int32, (count, count), 0) == lax.broadcasted_iota(
        jnp.int32, (count, count), 1
    )
    return jnp.sum(jnp.where(diagonal, column, 0.0), axis=0, keepdims=True)


def to_sublanes(row):
    count = row.shape[1]
    diagonal = lax.broadcasted_iota(jnp.int32, (count, count), 0) == lax.broadcasted_iota(
        jnp.int32, (count, count), 1
    )
    return jnp.sum(jnp.where(diagonal, row, 0.0), axis=1, keepdims=True)


def mix_kernel(
    n,
    t,
    mixout,
    tokens,
    gain_one,
    bias_one,
    gain_two,
    bias_two,
    w_out,
    w_up,
    w_down,
    out,
    out_buf,
    up_buf,
    down_buf,
    gathered,
    part,
    part_got,
    affine,
    firsts,
    normed,
    hidden,
    near_sent,
    near_got,
    kept,
    far_sent,
    far_got,
    stats,
    load_out,
    load_up,
    load_down,
    mix_send,
    mix_recv,
    part_send,
    part_recv,
    affine_send,
    affine_recv,
    first_send,
    first_recv,
    near_send,
    near_recv,
    far_send,
    far_recv,
    stats_send,
    stats_recv,
):
    kv, tp = lax.axis_index("kv"), lax.axis_index("tp")
    count, columns = out.shape
    rows = mixout.shape[0]
    group = n * t
    me = kv * t + tp
    width = group * columns
    offsets = [(o, u) for o in range(n) for u in range(t) if (o, u) != (0, 0)]

    def at(o, u):
        return {"kv": shifted(kv, o, n), "tp": shifted(tp, u, t)}

    def block(o, u):
        return shifted(kv, o, n) * t + shifted(tp, u, t)

    def columns_of(index):
        return pl.ds(pl.multiple_of(index * columns, columns), columns)

    wait_barrier = greet([at(o, u) for o, u in offsets])

    def load(source, target, sem):
        copy = pltpu.make_async_copy(source, target, sem)
        copy.start()
        return copy

    loads_out = [
        load(w_out.at[:, columns_of(shifted(tp, u, t))], out_buf.at[u], load_out.at[u])
        for u in range(t)
    ]
    up_chunks, _, up_width = up_buf.shape
    loads_up = [
        load(w_up.at[:, pl.ds(c * up_width, up_width)], up_buf.at[c], load_up.at[c])
        for c in range(up_chunks)
    ]
    steps = [*range(1, n), 0]
    loads_down = {
        (s, u): load(
            w_down.at[:, columns_of(block(steps[s], u))], down_buf.at[s, u], load_down.at[s, u]
        )
        for s in range(n)
        for u in range(t)
    }
    gathered[kv] = mixout[...]
    affine[me, 0:1] = gain_one[...]
    affine[me, 1:2] = bias_one[...]
    wait_barrier()
    pending = []

    mixes = [
        send(mixout, gathered.at[kv], mix_send.at[o], mix_recv.at[o], at(o, 0))
        for o in range(1, n)
    ]
    affines = [
        send(affine.at[me], affine.at[me], affine_send.at[o, u], affine_recv.at[o, u], at(o, u))
        for o, u in offsets
    ]
    pending += mixes + affines
    for copy in mixes:
        copy.wait_recv()
    whole = gathered[...].reshape(count, gathered.shape[2])
    parts = []
    for u in [*range(1, t), 0]:
        loads_out[u].wait()
        product = jnp.dot(whole, out_buf[u], preferred_element_type=jnp.float32)
        if u:
            part[u - 1] = product
            parts.append(
                send(
                    part.at[u - 1],
                    part_got.at[u - 1],
                    part_send.at[u - 1],
                    part_recv.at[u - 1],
                    at(0, u),
                )
            )
    pending += parts
    own_tokens = tokens[:, columns_of(tp)].astype(jnp.float32)
    first = residual_scale * own_tokens + product
    for u in range(1, t):
        parts[u - 1].wait_recv()
        first = first + part_got[u - 1]
    firsts[me] = first.astype(jnp.bfloat16)

    def pass_on(index, o, u):
        where = at(o, u) if u == 0 else at(0, u)
        copy = send(
            firsts.at[index], firsts.at[index], first_send.at[o, u], first_recv.at[o, u], where
        )
        pending.append(copy)
        return copy

    passed = {}
    for o in range(1, n):
        passed[o, 0] = pass_on(me, o, 0)
    for u in range(1, t):
        passed[0, u] = pass_on(me, 0, u)
    for copy in affines:
        copy.wait_recv()
    for o in range(1, n):
        passed[o, 0].wait_recv()
        for u in range(1, t):
            passed[o, u] = pass_on(block(n - o, 0), o, u)
    for o in range(n):
        for u in range(1, t):
            passed[o, u].wait_recv()

    total = jnp.zeros((count, 1), jnp.float32)
    for g in range(group):
        total = total + jnp.sum(firsts[g].astype(jnp.float32), axis=1, keepdims=True)
    center = total / width
    spread = jnp.zeros((count, 1), jnp.float32)
    for g in range(group):
        away = firsts[g].astype(jnp.float32) - center
        spread = spread + jnp.sum(away * away, axis=1, keepdims=True)
    scale = lax.rsqrt(spread / width + epsilon)

    def finish(values, pair):
        return ((values.astype(jnp.float32) - center) * scale * pair[0:1] + pair[1:2]).astype(
            jnp.bfloat16
        )

    for g in range(group):
        normed[:, g * columns : (g + 1) * columns] = finish(firsts[g], affine[g])
    own_normed = finish(firsts[me], affine[me])

    for c in range(up_chunks):
        loads_up[c].wait()
        upper = jnp.dot(normed[...], up_buf[c], preferred_element_type=jnp.float32)
        upper = jnp.maximum(upper, 0.0)
        hidden[:, c * up_width : (c + 1) * up_width] = (upper * upper).astype(jnp.bfloat16)

    near = {}
    far = {}

    def near_sum(s):
        value = kept[s]
        for u in range(1, t):
            near[s, u].wait_recv()
            value = value + near_got[s, u - 1].astype(jnp.float32)
        return value

    def far_out(s):
        far_sent[s] = near_sum(s).astype(jnp.bfloat16)
        far[s] = send(
            far_sent.at[s], far_got.at[s], far_send.at[s], far_recv.at[s], at(steps[s], 0)
        )

    for s in range(n):
        for u in [*range(1, t), 0]:
            loads_down[s, u].wait()
            product = jnp.dot(hidden[...], down_buf[s, u], preferred_element_type=jnp.float32)
            if u:
                near_sent[s, u - 1] = product.astype(jnp.bfloat16)
                near[s, u] = send(
                    near_sent.at[s, u - 1],
                    near_got.at[s, u - 1],
                    near_send.at[s, u - 1],
                    near_recv.at[s, u - 1],
                    at(0, u),
                )
            else:
                kept[s] = product
        if s:
            far_out(s - 1)
    second = residual_scale * own_normed.astype(jnp.float32) + near_sum(n - 1)
    for s in range(n - 1):
        far[s].wait_recv()
        second = second + far_got[s].astype(jnp.float32)
    pending += list(near.values()) + list(far.values())

    sums = jnp.concatenate(
        [
            to_lanes(jnp.sum(second, axis=1, keepdims=True)),
            to_lanes(jnp.sum(second * second, axis=1, keepdims=True)),
        ],
        axis=0,
    )
    stats[0, 0:2] = sums
    tallies = []
    for i, (o, u) in enumerate(offsets):
        tallies.append(
            send(stats.at[0], stats.at[i + 1], stats_send.at[i], stats_recv.at[i], at(o, u))
        )
    pending += tallies
    for i, copy in enumerate(tallies):
        copy.wait_recv()
        sums = sums + stats[i + 1, 0:2]
    center_two = to_sublanes(sums[0:1]) / width
    spread_two = to_sublanes(sums[1:2]) / width - center_two * center_two
    result = (second - center_two) * lax.rsqrt(spread_two + epsilon) * gain_two[...] + bias_two[...]
    out[...] = result.astype(jnp.bfloat16)
    for copy in pending:
        copy.wait_send()


def mix(mixout, tokens, affine, w_out, w_up, w_down, n, t):
    count = tokens.shape[0]
    rows, heads_width = mixout.shape
    columns = affine[0].shape[1]
    depth, units = w_up.shape
    group = n * t
    up_width = min(units, 512)
    dma = pltpu.SemaphoreType.DMA
    vmem = pltpu.VMEM
    few, many = jnp.bfloat16, jnp.float32
    return pl.pallas_call(
        functools.partial(mix_kernel, n, t),
        out_shape=jax.ShapeDtypeStruct((count, columns), few),
        in_specs=[pl.BlockSpec(memory_space=pltpu.VMEM)] * 6
        + [pl.BlockSpec(memory_space=pl.ANY)] * 3,
        out_specs=pl.BlockSpec(memory_space=pltpu.VMEM),
        scratch_shapes=[
            vmem((t, heads_width, columns), few),
            vmem((units // up_width, depth, up_width), few),
            vmem((n, t, units, columns), few),
            vmem((n, rows, heads_width), few),
            vmem((t - 1, count, columns), many),
            vmem((t - 1, count, columns), many),
            vmem((group, 2, columns), many),
            vmem((group, count, columns), few),
            vmem((count, depth), few),
            vmem((count, units), few),
            vmem((n, t - 1, count, columns), few),
            vmem((n, t - 1, count, columns), few),
            vmem((n, count, columns), many),
            vmem((n, count, columns), few),
            vmem((n, count, columns), few),
            vmem((group, 8, count), many),
            dma((t,)),
            dma((units // up_width,)),
            dma((n, t)),
            dma((n,)),
            dma((n,)),
            dma((t,)),
            dma((t,)),
            dma((n, t)),
            dma((n, t)),
            dma((n, t)),
            dma((n, t)),
            dma((n, t)),
            dma((n, t)),
            dma((n,)),
            dma((n,)),
            dma((group,)),
            dma((group,)),
        ],
        compiler_params=pltpu.CompilerParams(
            collective_id=1, has_side_effects=True, vmem_limit_bytes=VMEM_BYTES
        ),
        name="mix",
    )(mixout, tokens, *affine, w_out, w_up, w_down)


def per_device(
    tokens,
    state,
    w_query,
    w_forget,
    w_input,
    w_gate,
    lower_bound,
    head_gain,
    w_out,
    gain_one,
    bias_one,
    w_up,
    w_down,
    gain_two,
    bias_two,
):
    n, t = lax.axis_size("kv"), lax.axis_size("tp")
    size = head_gain.shape[0]
    columns, lines = project(
        tokens,
        lower_bound[None, :],
        (w_query, w_forget, w_input, w_gate),
        n,
        size,
    )
    new_state, mixout = update_state(state, columns, lines, head_gain[None, :])
    result = mix(
        mixout,
        tokens,
        [vector[None, :] for vector in (gain_one, bias_one, gain_two, bias_two)],
        w_out,
        w_up,
        w_down,
        n,
        t,
    )
    return (result, new_state)


def solution(mesh):
    placed = (
        P("dp", "kv"),
        P(("dp", "kv"), "tp", None, None),
        P("kv", "tp"),
        P("kv", "tp"),
        P("kv", "tp"),
        P("kv", "tp"),
        P("tp"),
        P(),
        P("tp", "kv"),
        P(("kv", "tp")),
        P(("kv", "tp")),
        P(None, ("kv", "tp")),
        P(("kv", "tp"), None),
        P(("kv", "tp")),
        P(("kv", "tp")),
    )
    return jax.shard_map(
        per_device,
        mesh=mesh,
        in_specs=placed,
        out_specs=(P("dp", ("kv", "tp")), P(("dp", "kv"), "tp", None, None)),
        check_vma=False,
    )
```

profile of v0, /device:TPU:0, one launch (start us, length us, event | category | flops | bytes accessed | tf_op | source)
XLA Modules:
  0.0 94.4 jit_solution(3268270017217212174)
XLA Ops:
  0.6 32.0 %project.1 = (bf16[3,32,64,32]{3,2,1,0:T(8,128)(2,1)}, f32[2,16,2048]{2,1,0:T(8,128)}) custom-call(bf16[64,1024]{1,0:T(8,128)(2,1)} %tokens.3, f32[1,2048]{1,0:T(1,128)} %bitcast.6, bf16[1024,2048]{1,0:T(8,128)(2,1)} %wq.1, bf16[1024,2048]{1,0:T(8,128)(2,1)} %wf.1, bf16[1024,2048]{1,0:T(8,128)(2,1)} %wi.1, bf16[1024,2048]{1,0:T(8,128)(2,1)} %wg.1), custom_call_target="tpu_custom_call" | custom-call | tf_op jit(solution)/shard_map/project/pallas_call | solution.py:126
  32.6 20.7 %state.2 = (f32[16,32,64,64]{3,2,1,0:T(8,128)}, bf16[16,2048]{1,0:T(8,128)(2,1)}) custom-call(f32[16,32,64,64]{3,2,1,0:T(8,128)} %state.3, bf16[3,32,64,32]{3,2,1,0:T(8,128)(2,1)} %get-tuple-element.6.columns, f32[2,16,2048]{2,1,0:T(8,128)} %get-tuple-element.7.lines, f32[1,64]{1,0:T(1,128)} %bitcast.11, bf16[32,2048]{1,0:T(8,128)(2,1)} %constant.2.clone.pick), custom_call_target="tpu_custom_call" | custom-call | tf_op jit(solution)/shard_map/state/pallas_call | solution.py:187
  53.4 39.5 %mix.1 = bf16[64,512]{1,0:T(8,128)(2,1)} custom-call(bf16[16,2048]{1,0:T(8,128)(2,1)} %get-tuple-element.8.mixout, bf16[64,1024]{1,0:T(8,128)(2,1)} %tokens.3, f32[1,512]{1,0:T(1,128)} %bitcast.7, f32[1,512]{1,0:T(1,128)} %bitcast.8, f32[1,512]{1,0:T(1,128)} %bitcast.9, f32[1,512]{1,0:T(1,128)} %bitcast.10, bf16[2048,1024]{1,0:T(8,128)(2,1)} %w_out.1, ...), custom_call_target="tpu_custom_call" | custom-call | tf_op jit(solution)/shard_map/mix/pallas_call | solution.py:482
  92.9 1.5 %copy.19 = bf16[64,512]{1,0:T(8,128)(2,1)} copy(bf16[64,512]{1,0:T(8,128)(2,1)} %mix.1) | data formatting | bytes 131072
where the time goes:
time: 95 us; the launch traced here: 94.4 us
  Pallas kernels  92.3 us (97%)
  local copies, waits for them, and re-layouts  1.47 us (2%)
    pallas_call x1, Pallas kernels, mix(): pl.pallas_call(functools.partial(mix_kernel, n, t), out_shape=jax.ShapeDt...  39.5 us
    pallas_call x1, Pallas kernels, project(): pl.pallas_call(functools.partial(project_kernel, n, chunk, size), out_sha...  32 us
    pallas_call x1, Pallas kernels, update_state(): pl.pallas_call(state_kernel, grid=(heads // some,), out_shape=(jax.ShapeD...  20.7 us

commit v1 on v0

v1 whole, which is shorter than its diff:
```python
import functools
import types

import jax
import jax.numpy as jnp
import numpy as np
from jax import lax
from jax.experimental import pallas as pl
from jax.experimental.pallas import tpu as pltpu
from jax.sharding import PartitionSpec as P

epsilon = 0.1
residual_scale = 1.68
MESH = pl.DeviceIdType.MESH
LAYER_BYTES = 47 * 1024 * 1024
WRITE_BYTES = 1024 * 1024


def shifted(index, by, count):
    return lax.rem(index + by, count)


def greet(peers):
    barrier = pltpu.get_barrier_semaphore()
    for peer in peers:
        pl.semaphore_signal(barrier, inc=1, device_id=peer, device_id_type=MESH)
    return lambda: pl.semaphore_wait(barrier, len(peers))


def send(source, target, send_sem, recv_sem, peer):
    copy = pltpu.make_async_remote_copy(
        src_ref=source,
        dst_ref=target,
        send_sem=send_sem,
        recv_sem=recv_sem,
        device_id=peer,
        device_id_type=MESH,
    )
    copy.start()
    return copy


def store(source, target, sem):
    copy = pltpu.make_async_copy(source, target, sem)
    copy.start()
    return copy


def to_lanes(column):
    count = column.shape[0]
    diagonal = lax.broadcasted_iota(jnp.int32, (count, count), 0) == lax.broadcasted_iota(
        jnp.int32, (count, count), 1
    )
    return jnp.sum(jnp.where(diagonal, column, 0.0), axis=0, keepdims=True)


def to_sublanes(row):
    count = row.shape[1]
    diagonal = lax.broadcasted_iota(jnp.int32, (count, count), 0) == lax.broadcasted_iota(
        jnp.int32, (count, count), 1
    )
    return jnp.sum(jnp.where(diagonal, row, 0.0), axis=1, keepdims=True)


def pick_matrix(rows, lanes):
    depth, width = 4 * rows, rows * 2 * lanes
    line = lax.broadcasted_iota(jnp.int32, (depth, width), 0)
    lane = lax.broadcasted_iota(jnp.int32, (depth, width), 1)
    same_row = lax.rem(line, rows) == lax.div(lane, 2 * lanes)
    same_half = (line < 2 * rows) == (lax.rem(lane, 2 * lanes) < lanes)
    return jnp.where(same_row & same_half, 1.0, 0.0).astype(jnp.bfloat16)


def layer_kernel(n, t, size, names, *refs):
    r = types.SimpleNamespace(**dict(zip(names, refs)))
    kv, tp = lax.axis_index("kv"), lax.axis_index("tp")
    count, columns = r.out.shape
    rows = count // n
    group = n * t
    me = kv * t + tp
    width = group * columns
    groups, kinds, _, _, wide = r.whole.shape
    heads = wide // size
    lanes = 2 * size
    pieces = r.down.shape[0] // group
    depth_down = r.down.shape[1]
    offsets = [(o, u) for o in range(n) for u in range(t) if (o, u) != (0, 0)]
    relay = n >= 4
    last = n - 1

    def at(o, u):
        return {"kv": shifted(kv, o, n), "tp": shifted(tp, u, t)}

    def block(o, u):
        return shifted(kv, o, n) * t + shifted(tp, u, t)

    def columns_of(index):
        return pl.ds(pl.multiple_of(index * columns, columns), columns)

    wait_barrier = greet([at(o, u) for o, u in offsets])

    small = [
        store(source, target, r.small_sem.at[i])
        for i, (source, target) in enumerate(
            [
                (r.tokens_in, r.tokens),
                (r.bound_in, r.bound),
                (r.gain_in, r.gain),
                (r.gain_one_in, r.gain_one),
                (r.bias_one_in, r.bias_one),
                (r.gain_two_in, r.gain_two),
                (r.bias_two_in, r.bias_two),
            ]
        )
    ]
    weights = (r.w_query, r.w_forget, r.w_input, r.w_gate)
    loads = {
        (j, w): store(
            weights[w].at[:, pl.ds(j * wide, wide)],
            r.pool.at[j * kinds + w],
            r.load_project.at[j * kinds + w],
        )
        for j in range(groups)
        for w in range(kinds)
    }

    r.pick[...] = pick_matrix(rows, lanes)
    if relay:

        @pl.when(kv == 0)
        def _():
            for j in range(groups):
                r.got[j, 0] = jnp.zeros(r.got.shape[2:], jnp.bfloat16)

        @pl.when(kv == last)
        def _():
            for j in range(groups):
                r.got[j, last - 1] = jnp.zeros(r.got.shape[2:], jnp.bfloat16)

    def guarded(condition, action):
        if condition is None:
            action()
        else:
            pl.when(condition)(action)

    sends = {}

    def direct(j, o):
        return pltpu.make_async_remote_copy(
            src_ref=r.sent.at[j, shifted(kv, o, n)],
            dst_ref=r.got.at[j, o - 1],
            send_sem=r.sum_send.at[j, o - 1],
            recv_sem=r.sum_recv.at[j, o - 1],
            device_id=at(o, 0),
            device_id_type=MESH,
        )

    def sends_direct(o):
        condition = None
        if relay:
            terms = []
            if o == 1:
                terms.append(kv != last)
            if o == last:
                terms.append(kv != 0)
            if o == last - 1:
                terms.append(kv != 1)
            if o == 2:
                terms.append(kv != last - 1)
            for term in terms:
                condition = term if condition is None else condition & term
        return condition

    def receives(o):
        if relay and o == 1:
            return kv != 0
        if relay and o == last:
            return kv != last
        return None

    is_end = (kv == 0) | (kv == last)
    is_relay = (kv == 1) | (kv == last - 1)

    def to_relay(j):
        return pltpu.make_async_remote_copy(
            src_ref=r.sent.at[j, last - kv],
            dst_ref=r.relay_got.at[j],
            send_sem=r.relay_send.at[j],
            recv_sem=r.relay_recv.at[j],
            device_id={"kv": 1 + (kv // last) * (last - 2), "tp": tp},
            device_id_type=MESH,
        )

    def from_relay(j):
        side = (kv - 1) // (last - 2)
        end = last - last * side
        slot = (last - 2) - (last - 3) * side
        return end, pltpu.make_async_remote_copy(
            src_ref=r.relay_sent.at[j],
            dst_ref=r.got.at[j, slot],
            send_sem=r.relay_send.at[j],
            recv_sem=r.sum_recv.at[j, slot],
            device_id={"kv": end, "tp": tp},
            device_id_type=MESH,
        )

    def project(j):
        for w in range(kinds):
            loads[j, w].wait()
            value = jnp.dot(
                r.tokens[...], r.pool[j * kinds + w], preferred_element_type=jnp.float32
            ).reshape(n, rows, wide)
            r.whole[j, w] = value
            r.sent[j, :, w] = value.astype(jnp.bfloat16)

    def send_far(j):
        if relay:
            pl.when(is_end)(lambda: to_relay(j).start())

    def send_near(j):
        for o in sorted(range(1, n), key=lambda o: -min(o, n - o)):
            guarded(sends_direct(o), lambda o=o: direct(j, o).start())

    def pass_relay(j):
        if not relay:
            return

        @pl.when(is_relay)
        def _():
            to_relay(j).wait_recv()
            end, copy = from_relay(j)
            for w in range(kinds):
                total = r.whole[j, w, end] + r.relay_got[j, w].astype(jnp.float32)
                r.relay_sent[j, w] = total.astype(jnp.bfloat16)
            copy.start()

    def finish_sends(j):
        for o in range(1, n):
            guarded(sends_direct(o), lambda o=o: direct(j, o).wait_send())
        if relay:
            pl.when(is_end)(lambda: to_relay(j).wait_send())
            pl.when(is_relay)(lambda: from_relay(j)[1].wait_send())

    def load_state(j):
        part = pl.ds(j * heads, heads)
        return store(r.state.at[:, part], r.new_state.at[:, part], r.load_state.at[j])

    pending = []

    def update(j):
        for o in range(1, n):
            guarded(receives(o), lambda o=o: direct(j, o).wait_recv())

        def summed(w):
            total = r.whole[j, w, kv]
            for o in range(1, n):
                total = total + r.got[j, o - 1, w].astype(jnp.float32)
            return total.astype(jnp.bfloat16).astype(jnp.float32)

        query_raw, forget_raw, value, gate = (summed(w) for w in range(kinds))
        low = r.bound[:, j * wide : (j + 1) * wide]
        forget = low + (1.0 - low) * jax.nn.sigmoid(forget_raw)
        query = query_raw * jax.nn.sigmoid(query_raw)
        stacked = []
        for factor in (forget, query):
            high = factor.astype(jnp.bfloat16).astype(jnp.float32)
            stacked += [high, factor - high]
        turned = jnp.concatenate(stacked, axis=0).T.reshape(heads, size, 4 * rows)
        r.factors[...] = turned.astype(jnp.bfloat16)
        for h in range(heads):
            pair = value[:, (h // 2) * lanes : (h // 2 + 1) * lanes]
            r.value[h] = pltpu.roll(pair, size, 1) if h % 2 else pair
        r.gate[...] = gate * jax.nn.sigmoid(gate)
        state_loads[j].wait()

        def one_head(h, slot):
            r.spread[slot] = jnp.dot(
                r.factors[h], r.pick[...], preferred_element_type=jnp.float32
            )
            for b in range(rows):
                base = b * 2 * lanes
                line = r.value[h, b : b + 1, :size]
                keep = r.spread[slot, :, base : base + size]
                query_column = r.spread[slot, :, base + lanes : base + lanes + size]
                updated = line + keep * (r.new_state[b, j * heads + h] - line)
                r.new_state[b, j * heads + h] = updated
                r.read[h, b : b + 1] = jnp.sum(updated * query_column, axis=0, keepdims=True)

        def two_heads(i, carry):
            for slot in range(2):
                one_head(i * 2 + slot, slot)
            return carry

        lax.fori_loop(0, heads // 2, two_heads, 0)

        def normalized(h):
            whole = r.read[h]
            return whole * lax.rsqrt(jnp.mean(whole * whole, axis=1, keepdims=True) + epsilon)

        for p in range(heads // 2):
            here = slice(p * lanes, (p + 1) * lanes)
            pair = jnp.concatenate([normalized(2 * p), normalized(2 * p + 1)], axis=1)
            gated = pair * r.gain[...] * r.gate[:, here]
            r.gathered[j, kv, :, here] = gated.astype(jnp.bfloat16)
        for o in range(1, n):
            mixes[j, o] = send(
                r.gathered.at[j, kv],
                r.gathered.at[j, kv],
                r.mix_send.at[j, o],
                r.mix_recv.at[j, o],
                at(o, 0),
            )
            pending.append(mixes[j, o])

    mixes = {}

    def project_out(j):
        for o in range(1, n):
            mixes[j, o].wait_recv()
        whole = r.gathered[j].reshape(count, wide)
        for u in range(t):
            if j == 0:
                loads_out[u].wait()
            product = jnp.dot(
                whole,
                r.out_buf[u, j * wide : (j + 1) * wide],
                preferred_element_type=jnp.float32,
            )
            r.mixed[u] = product if j == 0 else r.mixed[u] + product

    small[0].wait()
    state_loads = {}
    for j in range(groups):
        project(j)
        if j == 0:
            wait_barrier()
        send_far(j)
        send_near(j)
        state_loads[j] = load_state(j)
    for copy in small[1:]:
        copy.wait()
    loads_out = [
        store(r.w_out.at[:, columns_of(shifted(tp, u, t))], r.out_buf.at[u], r.load_out.at[u])
        for u in range(t)
    ]
    up_chunks, _, up_width = r.up_buf.shape
    loads_up = [
        store(r.w_up.at[:, pl.ds(c * up_width, up_width)], r.up_buf.at[c], r.load_up.at[c])
        for c in range(up_chunks)
    ]
    steps = [*range(1, n), 0]
    loads_down = {}
    for s in range(n):
        for u in [*range(1, t), 0]:
            for p in range(pieces):
                slot = (s * t + u) * pieces + p
                loads_down[s, u, p] = store(
                    r.w_down.at[pl.ds(p * depth_down, depth_down), columns_of(block(steps[s], u))],
                    r.down.at[slot],
                    r.load_down.at[slot],
                )

    r.affine[me, 0:1] = r.gain_one[...]
    r.affine[me, 1:2] = r.bias_one[...]
    affines = [
        send(
            r.affine.at[me], r.affine.at[me], r.affine_send.at[o, u], r.affine_recv.at[o, u], at(o, u)
        )
        for o, u in offsets
    ]
    pending += affines

    for j in range(groups):
        pass_relay(j)
        update(j)
        if j:
            project_out(j - 1)
    project_out(groups - 1)

    parts = []
    for u in range(1, t):
        parts.append(
            send(
                r.mixed.at[u],
                r.part_got.at[u - 1],
                r.part_send.at[u],
                r.part_recv.at[u],
                at(0, u),
            )
        )
    pending += parts
    own_tokens = r.tokens[:, columns_of(tp)].astype(jnp.float32)
    first = residual_scale * own_tokens + r.mixed[0]
    for u in range(1, t):
        parts[u - 1].wait_recv()
        first = first + r.part_got[u - 1]
    r.firsts[me] = first.astype(jnp.bfloat16)

    def pass_on(index, o, u):
        where = at(o, u) if u == 0 else at(0, u)
        copy = send(
            r.firsts.at[index], r.firsts.at[index], r.first_send.at[o, u], r.first_recv.at[o, u], where
        )
        pending.append(copy)
        return copy

    passed = {}
    for o in range(1, n):
        passed[o, 0] = pass_on(me, o, 0)
    for u in range(1, t):
        passed[0, u] = pass_on(me, 0, u)
    for copy in affines:
        copy.wait_recv()
    for o in range(1, n):
        passed[o, 0].wait_recv()
        for u in range(1, t):
            passed[o, u] = pass_on(block(n - o, 0), o, u)
    for o in range(n):
        for u in range(1, t):
            passed[o, u].wait_recv()

    total = jnp.zeros((count, 1), jnp.float32)
    for g in range(group):
        total = total + jnp.sum(r.firsts[g].astype(jnp.float32), axis=1, keepdims=True)
    center = total / width
    spread = jnp.zeros((count, 1), jnp.float32)
    for g in range(group):
        away = r.firsts[g].astype(jnp.float32) - center
        spread = spread + jnp.sum(away * away, axis=1, keepdims=True)
    scale = lax.rsqrt(spread / width + epsilon)

    def finish(values, pair):
        return ((values.astype(jnp.float32) - center) * scale * pair[0:1] + pair[1:2]).astype(
            jnp.bfloat16
        )

    for g in range(group):
        r.normed[:, g * columns : (g + 1) * columns] = finish(r.firsts[g], r.affine[g])
    own_normed = finish(r.firsts[me], r.affine[me])

    for c in range(up_chunks):
        loads_up[c].wait()
        upper = jnp.dot(r.normed[...], r.up_buf[c], preferred_element_type=jnp.float32)
        upper = jnp.maximum(upper, 0.0)
        r.hidden[:, c * up_width : (c + 1) * up_width] = (upper * upper).astype(jnp.bfloat16)

    near = {}
    far = {}

    def near_sum(s):
        value = r.kept[s]
        for u in range(1, t):
            near[s, u].wait_recv()
            value = value + r.near_got[s, u - 1].astype(jnp.float32)
        return value

    def far_out(s):
        r.far_sent[s] = near_sum(s).astype(jnp.bfloat16)
        far[s] = send(
            r.far_sent.at[s], r.far_got.at[s], r.far_send.at[s], r.far_recv.at[s], at(steps[s], 0)
        )

    for s in range(n):
        for u in [*range(1, t), 0]:
            product = jnp.zeros((count, columns), jnp.float32)
            for p in range(pieces):
                loads_down[s, u, p].wait()
                product = product + jnp.dot(
                    r.hidden[:, p * depth_down : (p + 1) * depth_down],
                    r.down[(s * t + u) * pieces + p],
                    preferred_element_type=jnp.float32,
                )
            if u:
                r.near_sent[s, u - 1] = product.astype(jnp.bfloat16)
                near[s, u] = send(
                    r.near_sent.at[s, u - 1],
                    r.near_got.at[s, u - 1],
                    r.near_send.at[s, u - 1],
                    r.near_recv.at[s, u - 1],
                    at(0, u),
                )
            else:
                r.kept[s] = product
        if s:
            far_out(s - 1)
    second = residual_scale * own_normed.astype(jnp.float32) + near_sum(n - 1)
    for s in range(n - 1):
        far[s].wait_recv()
        second = second + r.far_got[s].astype(jnp.float32)
    pending += list(near.values()) + list(far.values())

    sums = jnp.concatenate(
        [
            to_lanes(jnp.sum(second, axis=1, keepdims=True)),
            to_lanes(jnp.sum(second * second, axis=1, keepdims=True)),
        ],
        axis=0,
    )
    r.stats[0, 0:2] = sums
    tallies = []
    for i, (o, u) in enumerate(offsets):
        tallies.append(
            send(r.stats.at[0], r.stats.at[i + 1], r.stats_send.at[i], r.stats_recv.at[i], at(o, u))
        )
    pending += tallies
    for i, copy in enumerate(tallies):
        copy.wait_recv()
        sums = sums + r.stats[i + 1, 0:2]
    center_two = to_sublanes(sums[0:1]) / width
    spread_two = to_sublanes(sums[1:2]) / width - center_two * center_two
    result = (second - center_two) * lax.rsqrt(spread_two + epsilon)
    r.out[...] = (result * r.gain_two[...] + r.bias_two[...]).astype(jnp.bfloat16)
    for j in range(groups):
        finish_sends(j)
    for copy in pending:
        copy.wait_send()


def layer(n, t, tokens, state, weights, bound, gain, w_out, w_up, w_down, affine):
    count, depth = tokens.shape
    rows = count // n
    width = weights[0].shape[1]
    kinds = len(weights)
    size = state.shape[3]
    lanes = 2 * size
    wide = min(width, 8 * size)
    groups = width // wide
    heads = wide // size
    columns = affine[0].shape[1]
    model, units = w_up.shape
    group = n * t
    up_width = min(units, 512)
    dma = pltpu.SemaphoreType.DMA
    vmem = pltpu.VMEM
    few, many = jnp.bfloat16, jnp.float32
    shares = columns == wide and units % depth == 0 and group * (units // depth) == groups * kinds
    pieces = units // depth if shares else 1
    inputs = {
        "tokens_in": tokens,
        "state": state,
        "w_query": weights[0],
        "w_forget": weights[1],
        "w_input": weights[2],
        "w_gate": weights[3],
        "bound_in": bound,
        "gain_in": gain,
        "w_out": w_out,
        "w_up": w_up,
        "w_down": w_down,
        "gain_one_in": affine[0],
        "bias_one_in": affine[1],
        "gain_two_in": affine[2],
        "bias_two_in": affine[3],
    }
    scratch = {
        "tokens": vmem(tokens.shape, few),
        "bound": vmem(bound.shape, many),
        "gain": vmem(gain.shape, many),
        "gain_one": vmem((1, columns), many),
        "bias_one": vmem((1, columns), many),
        "gain_two": vmem((1, columns), many),
        "bias_two": vmem((1, columns), many),
        "pool": vmem((groups * kinds, depth, wide), few),
        "whole": vmem((groups, kinds, n, rows, wide), many),
        "sent": vmem((groups, n, kinds, rows, wide), few),
        "got": vmem((groups, n - 1, kinds, rows, wide), few),
        "relay_got": vmem((groups, kinds, rows, wide), few),
        "relay_sent": vmem((groups, kinds, rows, wide), few),
        "pick": vmem((4 * rows, rows * 2 * lanes), few),
        "factors": vmem((heads, size, 4 * rows), few),
        "value": vmem((heads, rows, lanes), many),
        "gate": vmem((rows, wide), many),
        "spread": vmem((2, size, rows * 2 * lanes), many),
        "read": vmem((heads, rows, size), many),
        "gathered": vmem((groups, n, rows, wide), few),
        "out_buf": vmem((t, width, columns), few),
        "mixed": vmem((t, count, columns), many),
        "up_buf": vmem((units // up_width, model, up_width), few),
        "part_got": vmem((t - 1, count, columns), many),
        "affine": vmem((group, 2, columns), many),
        "firsts": vmem((group, count, columns), few),
        "normed": vmem((count, model), few),
        "hidden": vmem((count, units), few),
        "near_sent": vmem((n, t - 1, count, columns), few),
        "near_got": vmem((n, t - 1, count, columns), few),
        "kept": vmem((n, count, columns), many),
        "far_sent": vmem((n, count, columns), few),
        "far_got": vmem((n, count, columns), few),
        "stats": vmem((group, 8, count), many),
        "small_sem": dma((7,)),
        "load_project": dma((groups * kinds,)),
        "load_state": dma((groups,)),
        "load_out": dma((t,)),
        "load_up": dma((units // up_width,)),
        "load_down": dma((group * pieces,)),
        "sum_send": dma((groups, n - 1)),
        "sum_recv": dma((groups, n - 1)),
        "relay_send": dma((groups,)),
        "relay_recv": dma((groups,)),
        "mix_send": dma((groups, n)),
        "mix_recv": dma((groups, n)),
        "part_send": dma((t,)),
        "part_recv": dma((t,)),
        "affine_send": dma((n, t)),
        "affine_recv": dma((n, t)),
        "first_send": dma((n, t)),
        "first_recv": dma((n, t)),
        "near_send": dma((n, t)),
        "near_recv": dma((n, t)),
        "far_send": dma((n,)),
        "far_recv": dma((n,)),
        "stats_send": dma((group,)),
        "stats_recv": dma((group,)),
    }
    if not shares:
        scratch["down"] = vmem((group, units, columns), few)

    def kernel(*refs):
        names = [*inputs, "out", "new_state", *scratch]
        if shares:
            names.append("down")
            refs = (*refs, refs[names.index("pool")])
        layer_kernel(n, t, size, names, *refs)

    return pl.pallas_call(
        kernel,
        out_shape=(vmem((count, columns), few), vmem(state.shape, many)),
        in_specs=[pl.BlockSpec(memory_space=pl.ANY)] * len(inputs),
        out_specs=(pl.BlockSpec(memory_space=pltpu.VMEM),) * 2,
        scratch_shapes=list(scratch.values()),
        compiler_params=pltpu.CompilerParams(
            collective_id=0, has_side_effects=True, vmem_limit_bytes=LAYER_BYTES
        ),
        name="layer",
    )(*inputs.values())


def write_kernel(result, new_state, result_out, state_out, sem):
    pieces = sem.shape[0] - 1
    heads = new_state.shape[1] // pieces
    copies = [store(result, result_out, sem.at[pieces])]
    for i in range(pieces):
        part = pl.ds(i * heads, heads)
        copies.append(store(new_state.at[:, part], state_out.at[:, part], sem.at[i]))
    for copy in copies:
        copy.wait()


def write_out(result, new_state):
    return pl.pallas_call(
        write_kernel,
        out_shape=(
            jax.ShapeDtypeStruct(result.shape, result.dtype),
            jax.ShapeDtypeStruct(new_state.shape, new_state.dtype),
        ),
        in_specs=[pl.BlockSpec(memory_space=pltpu.VMEM)] * 2,
        out_specs=(pl.BlockSpec(memory_space=pl.ANY),) * 2,
        scratch_shapes=[pltpu.SemaphoreType.DMA((9,))],
        compiler_params=pltpu.CompilerParams(vmem_limit_bytes=WRITE_BYTES),
        name="write",
    )(result, new_state)


def per_device(
    tokens,
    state,
    w_query,
    w_forget,
    w_input,
    w_gate,
    lower_bound,
    head_gain,
    w_out,
    gain_one,
    bias_one,
    w_up,
    w_down,
    gain_two,
    bias_two,
):
    n, t = lax.axis_size("kv"), lax.axis_size("tp")
    result, new_state = layer(
        n,
        t,
        tokens,
        state,
        (w_query, w_forget, w_input, w_gate),
        lower_bound[None, :],
        jnp.tile(head_gain, 2)[None, :],
        w_out,
        w_up,
        w_down,
        [vector[None, :] for vector in (gain_one, bias_one, gain_two, bias_two)],
    )
    return write_out(result, new_state)


def solution(mesh):
    placed = (
        P("dp", "kv"),
        P(("dp", "kv"), "tp", None, None),
        P("kv", "tp"),
        P("kv", "tp"),
        P("kv", "tp"),
        P("kv", "tp"),
        P("tp"),
        P(),
        P("tp", "kv"),
        P(("kv", "tp")),
        P(("kv", "tp")),
        P(None, ("kv", "tp")),
        P(("kv", "tp"), None),
        P(("kv", "tp")),
        P(("kv", "tp")),
    )
    return jax.shard_map(
        per_device,
        mesh=mesh,
        in_specs=placed,
        out_specs=(P("dp", ("kv", "tp")), P(("dp", "kv"), "tp", None, None)),
        check_vma=False,
    )
```

time: 95 us -> 78.1 us (0.82)
  Pallas kernels: 92.3 us -> 76.1 us
    pallas_call x3 -> x2, Pallas kernels: 92.3 us -> 76.1 us  [the longest x1 70.1 us: layer(): pl.pallas_call(kernel, out_shape=(vmem((count, columns), few), vmem(state...]
    unnamed x1 -> x0, local copies, waits for them, and re-layouts: 1.47 us -> none
    another operation x0 -> x2, local copies, waits for them, and re-layouts: none -> 1.25 us  [per_device(): jnp.tile(head_gain, 2)[None, :]]
where the time goes in v1:
time: 78.1 us; the launch traced here: 78 us
  Pallas kernels  76.1 us (97%)
  local copies, waits for them, and re-layouts  1.25 us (2%)
    pallas_call x1, Pallas kernels, layer(): pl.pallas_call(kernel, out_shape=(vmem((count, columns), few), vmem(state...  70.1 us
    pallas_call x1, Pallas kernels, write_out(): pl.pallas_call(write_kernel, out_shape=(jax.ShapeDtypeStruct(result.shape...  5.95 us

profile of v1, /device:TPU:0, one launch (start us, length us, event | category | flops | bytes accessed | tf_op | source)
XLA Modules:
  0.0 78.0 jit_solution(10463895745581792098)
XLA Ops:
  0.6 0.7 tile.2
  1.3 0.6 broadcast_in_dim_tile.3.refs_7_
  1.9 70.1 %layer.1 = (bf16[64,512]{1,0:T(8,128)(2,1)S(1)}, f32[16,32,64,64]{3,2,1,0:T(8,128)S(1)}) custom-call(bf16[64,1024]{1,0:T(8,128)(2,1)} %refs_0_.1, f32[16,32,64,64]{3,2,1,0:T(8,128)} %refs_1_.1, bf16[1024,2048]{1,0:T(8,128)(2,1)} %refs_2_.1, bf16[1024,2048]{1,0:T(8,128)(2,1)} %refs_3_.1, bf16[1024,2048]{1,0:T(8,128)(2,1)} %refs_4_.1, ...), custom_call_target="tpu_custom_call" | custom-call | tf_op jit(solution)/shard_map/layer/pallas_call | solution.py:625
  72.0 6.0 %write.1 = (bf16[64,512]{1,0:T(8,128)(2,1)}, f32[16,32,64,64]{3,2,1,0:T(8,128)}) custom-call(bf16[64,512]{1,0:T(8,128)(2,1)S(1)} %get-tuple-element.4.result, f32[16,32,64,64]{3,2,1,0:T(8,128)S(1)} %get-tuple-element.5.new_state), custom_call_target="tpu_custom_call" | custom-call | tf_op jit(solution)/shard_map/write/pallas_call | solution.py:650

commit v2 on v1

v2 whole, which is shorter than its diff:
```python
import functools
import types

import jax
import jax.numpy as jnp
import numpy as np
from jax import lax
from jax.experimental import pallas as pl
from jax.experimental.pallas import tpu as pltpu
from jax.sharding import PartitionSpec as P

epsilon = 0.1
residual_scale = 1.68
MESH = pl.DeviceIdType.MESH
LAYER_BYTES = 47 * 1024 * 1024
WRITE_BYTES = 1024 * 1024


def shifted(index, by, count):
    return lax.rem(index + by, count)


def greet(peers):
    barrier = pltpu.get_barrier_semaphore()
    for peer in peers:
        pl.semaphore_signal(barrier, inc=1, device_id=peer, device_id_type=MESH)
    return lambda: pl.semaphore_wait(barrier, len(peers))


def send(source, target, send_sem, recv_sem, peer):
    copy = pltpu.make_async_remote_copy(
        src_ref=source,
        dst_ref=target,
        send_sem=send_sem,
        recv_sem=recv_sem,
        device_id=peer,
        device_id_type=MESH,
    )
    copy.start()
    return copy


def store(source, target, sem):
    copy = pltpu.make_async_copy(source, target, sem)
    copy.start()
    return copy


def to_lanes(column):
    count = column.shape[0]
    diagonal = lax.broadcasted_iota(jnp.int32, (count, count), 0) == lax.broadcasted_iota(
        jnp.int32, (count, count), 1
    )
    return jnp.sum(jnp.where(diagonal, column, 0.0), axis=0, keepdims=True)


def to_sublanes(row):
    count = row.shape[1]
    diagonal = lax.broadcasted_iota(jnp.int32, (count, count), 0) == lax.broadcasted_iota(
        jnp.int32, (count, count), 1
    )
    return jnp.sum(jnp.where(diagonal, row, 0.0), axis=1, keepdims=True)


def fill_pick(pick, rows, lanes):
    shape = (4 * rows, 2 * lanes)
    line = lax.broadcasted_iota(jnp.int32, shape, 0)
    lane = lax.broadcasted_iota(jnp.int32, shape, 1)
    same_half = (line < 2 * rows) == (lane < lanes)
    row = lax.rem(line, rows)
    for b in range(rows):
        chosen = jnp.where(same_half & (row == b), 1.0, 0.0)
        pick[:, b * 2 * lanes : (b + 1) * 2 * lanes] = chosen.astype(jnp.bfloat16)


def layer_kernel(n, t, size, names, *refs):
    r = types.SimpleNamespace(**dict(zip(names, refs)))
    kv, tp = lax.axis_index("kv"), lax.axis_index("tp")
    count, columns = r.out.shape
    rows = count // n
    group = n * t
    me = kv * t + tp
    width = group * columns
    groups, kinds, _, _, wide = r.whole.shape
    heads = wide // size
    lanes = 2 * size
    pieces = r.down.shape[0] // group
    depth_down = r.down.shape[1]
    offsets = [(o, u) for o in range(n) for u in range(t) if (o, u) != (0, 0)]
    relay = n == 4
    buddy = kv + 1 - 2 * lax.rem(kv, 2)

    def at(o, u):
        return {"kv": shifted(kv, o, n), "tp": shifted(tp, u, t)}

    def block(o, u):
        return shifted(kv, o, n) * t + shifted(tp, u, t)

    arrivals = sorted(range(1, n), key=lambda o: min(o, n - o))
    if relay:
        arrivals = [2, 3 - 2 * (kv // 2), 1 + 2 * (kv // 2)]

    def columns_of(index):
        return pl.ds(pl.multiple_of(index * columns, columns), columns)

    barrier = pltpu.get_barrier_semaphore()

    def greet_all():
        for o, u in offsets:
            pl.semaphore_signal(barrier, inc=1, device_id=at(o, u), device_id_type=MESH)

    def wait_barrier():
        pl.semaphore_wait(barrier, len(offsets))

    small = []

    def load_small(pairs):
        for source, target in pairs:
            small.append(store(source, target, r.small_sem.at[len(small)]))

    weights = (r.w_query, r.w_forget, r.w_input, r.w_gate)
    loads = {}

    def load_weights(j):
        for w in range(kinds):
            loads[j, w] = store(
                weights[w].at[:, pl.ds(j * wide, wide)],
                r.pool.at[j * kinds + w],
                r.load_project.at[j * kinds + w],
            )

    def wait_tokens():
        small[0].wait()

    def fill():
        fill_pick(r.pick, rows, lanes)
        if relay:

            @pl.when(is_end)
            def _():
                r.far_got[3 - kv] = jnp.zeros(r.far_got.shape[1:], jnp.bfloat16)

    def guarded(condition, action):
        if condition is None:
            action()
        else:
            pl.when(condition)(action)

    def direct(j, o):
        slot = 1 if relay else o - 1
        where = buddy if relay else shifted(kv, o, n)
        return pltpu.make_async_remote_copy(
            src_ref=r.sent.at[j, where],
            dst_ref=r.got.at[j, slot],
            send_sem=r.sum_send.at[j, slot],
            recv_sem=r.sum_recv.at[j, slot],
            device_id={"kv": where, "tp": tp},
            device_id_type=MESH,
        )

    reach = (1,) if relay else tuple(range(1, n))

    vectors = [
        (r.bound_in, r.bound),
        (r.gain_in, r.gain),
        (r.gain_one_in, r.gain_one),
        (r.bias_one_in, r.bias_one),
        (r.gain_two_in, r.gain_two),
        (r.bias_two_in, r.bias_two),
    ]
    is_end = (kv == 0) | (kv == n - 1)
    is_relay = (kv != 0) & (kv != n - 1)
    lead = min(2, groups)

    def to_relay(j, i):
        return pltpu.make_async_remote_copy(
            src_ref=r.sent.at[j, 3 - (buddy if i else kv)],
            dst_ref=r.relay_got.at[j, i],
            send_sem=r.relay_send.at[j, i],
            recv_sem=r.relay_recv.at[j, i],
            device_id={"kv": buddy, "tp": tp},
            device_id_type=MESH,
        )

    def from_relay(j, i):
        target = 3 - (kv if i else buddy)
        return target, pltpu.make_async_remote_copy(
            src_ref=r.relay_sent.at[j, i],
            dst_ref=r.got.at[j, 0],
            send_sem=r.relay_send.at[j, i],
            recv_sem=r.sum_recv.at[j, 0],
            device_id={"kv": target, "tp": tp},
            device_id_type=MESH,
        )

    def project(j):
        for w in range(kinds):
            loads[j, w].wait()
            value = jnp.dot(
                r.tokens[...], r.pool[j * kinds + w], preferred_element_type=jnp.float32
            ).reshape(n, rows, wide)
            r.whole[j, w] = value
            r.sent[j, :, w] = value.astype(jnp.bfloat16)

    def send_far(j):
        if relay:

            @pl.when(is_end)
            def _():
                for i in range(2):
                    to_relay(j, i).start()

    def send_near(j, chosen):
        def start():
            for o in reach:
                direct(j, o).start()

        guarded(chosen, start)

    def pass_relay(j):
        if not relay:
            return

        @pl.when(is_relay)
        def _():
            for i in range(2):
                to_relay(j, i).wait_recv()
                target, copy = from_relay(j, i)
                for w in range(kinds):
                    total = r.whole[j, w, target] + r.relay_got[j, i, w].astype(jnp.float32)
                    r.relay_sent[j, i, w] = total.astype(jnp.bfloat16)
                copy.start()

    def finish_sends(j):
        for o in reach:
            direct(j, o).wait_send()
        if relay:
            for i in range(2):
                to_relay(j, i).wait_send()

    def load_state(j):
        part = pl.ds(j * heads, heads)
        state_loads[j] = store(r.state.at[:, part], r.new_state.at[:, part], r.load_state.at[j])

    pending = []

    def wait_sums(j):
        if relay:
            from_relay(j, 0)[1].wait_recv()
        for o in reach:
            direct(j, o).wait_recv()

    def prepare(j):
        def summed(w):
            total = r.whole[j, w, kv]
            for slot in range(r.got.shape[1]):
                total = total + r.got[j, slot, w].astype(jnp.float32)
            return total.astype(jnp.bfloat16).astype(jnp.float32)

        query_raw, forget_raw, value, gate = (summed(w) for w in range(kinds))
        low = r.bound[:, j * wide : (j + 1) * wide]
        forget = low + (1.0 - low) * jax.nn.sigmoid(forget_raw)
        query = query_raw * jax.nn.sigmoid(query_raw)
        stacked = []
        for factor in (forget, query):
            high = factor.astype(jnp.bfloat16).astype(jnp.float32)
            stacked += [high, factor - high]
        turned = jnp.concatenate(stacked, axis=0).T.reshape(heads, size, 4 * rows)
        r.factors[...] = turned.astype(jnp.bfloat16)
        for h in range(heads):
            pair = value[:, (h // 2) * lanes : (h // 2 + 1) * lanes]
            r.value[h] = pltpu.roll(pair, size, 1) if h % 2 else pair
        r.gate[...] = gate * jax.nn.sigmoid(gate)

    def update(j):
        state_loads[j].wait()

        def one_head(h, slot):
            r.spread[slot] = jnp.dot(
                r.factors[h], r.pick[...], preferred_element_type=jnp.float32
            )
            for b in range(rows):
                base = b * 2 * lanes
                line = r.value[h, b : b + 1, :size]
                keep = r.spread[slot, :, base : base + size]
                query_column = r.spread[slot, :, base + lanes : base + lanes + size]
                updated = line + keep * (r.new_state[b, j * heads + h] - line)
                r.new_state[b, j * heads + h] = updated
                r.read[h, b : b + 1] = jnp.sum(updated * query_column, axis=0, keepdims=True)

        def two_heads(i, carry):
            for slot in range(2):
                one_head(i * 2 + slot, slot)
            return carry

        lax.fori_loop(0, heads // 2, two_heads, 0)

    def gated_out(j):
        def normalized(h):
            whole = r.read[h]
            return whole * lax.rsqrt(jnp.mean(whole * whole, axis=1, keepdims=True) + epsilon)

        for p in range(heads // 2):
            here = slice(p * lanes, (p + 1) * lanes)
            pair = jnp.concatenate([normalized(2 * p), normalized(2 * p + 1)], axis=1)
            gated = pair * r.gain[...] * r.gate[:, here]
            r.gathered[j, kv, :, here] = gated.astype(jnp.bfloat16)
        for o in range(1, n):
            guarded(sends_mix(j, o), mix_copy(j, o).start)

    def mix_copy(j, o):
        return pltpu.make_async_remote_copy(
            src_ref=r.gathered.at[j, kv],
            dst_ref=r.gathered.at[j, kv],
            send_sem=r.mix_send.at[j, o],
            recv_sem=r.mix_recv.at[j, o],
            device_id=at(o, 0),
            device_id_type=MESH,
        )

    def hops(j):
        return relay and j < groups - 1

    def sends_mix(j, o):
        return (kv != 3 if o == 1 else kv != 0 if o == 3 else is_relay) if hops(j) else None

    def forward_mix(j, i):
        return pltpu.make_async_remote_copy(
            src_ref=r.gathered.at[j, buddy],
            dst_ref=r.gathered.at[j, buddy],
            send_sem=r.mix_forward.at[j, i],
            recv_sem=r.mix_recv.at[j, 5 - 2 * kv if i else 2],
            device_id={"kv": 3 - (buddy if i else kv), "tp": tp},
            device_id_type=MESH,
        )

    def forward_mixes(j):
        if not hops(j):
            return

        @pl.when(is_relay)
        def _():
            pltpu.make_async_remote_copy(
                src_ref=r.gathered.at[j, kv],
                dst_ref=r.gathered.at[j, buddy],
                send_sem=r.mix_send.at[j, 1],
                recv_sem=r.mix_recv.at[j, 2 * kv - 1],
                device_id={"kv": buddy, "tp": tp},
                device_id_type=MESH,
            ).wait_recv()
            for i in range(2):
                forward_mix(j, i).start()

    def finish_mixes(j):
        for o in range(1, n):
            guarded(sends_mix(j, o), mix_copy(j, o).wait_send)
        if hops(j):

            @pl.when(is_relay)
            def _():
                for i in range(2):
                    forward_mix(j, i).wait_send()

    def wait_mixes(j):
        for o in range(1, n):
            condition = None
            if hops(j) and o != 2:
                condition = kv != (1 if o == 1 else 2)
            guarded(condition, mix_copy(j, o).wait_recv)

    def project_out(j):
        whole = r.gathered[j].reshape(count, wide)
        for u in range(t):
            if j == 0:
                loads_out[u].wait()
            product = jnp.dot(
                whole,
                r.out_buf[u, j * wide : (j + 1) * wide],
                preferred_element_type=jnp.float32,
            )
            r.mixed[u] = product if j == 0 else r.mixed[u] + product

    loads_out, loads_up, loads_down, state_loads = {}, {}, {}, {}
    up_chunks, _, up_width = r.up_buf.shape
    dests = [shifted(kv, o, n) for o in [*range(1, n), 0]]
    if relay:
        tables = [(3, 2, 1, 0), (2, 0, 3, 1), (1, 3, 0, 2), (0, 1, 2, 3)]
        dests = [
            jnp.where(kv < 2, jnp.where(kv == 0, a, b), jnp.where(kv == 2, c, d))
            for a, b, c, d in zip(*tables)
        ]

    def load_rest():
        for u in range(t):
            loads_out[u] = store(
                r.w_out.at[:, columns_of(shifted(tp, u, t))], r.out_buf.at[u], r.load_out.at[u]
            )
        for c in range(up_chunks):
            loads_up[c] = store(
                r.w_up.at[:, pl.ds(c * up_width, up_width)], r.up_buf.at[c], r.load_up.at[c]
            )
        for s in range(n):
            for u in [*range(1, t), 0]:
                for p in range(pieces):
                    slot = (s * t + u) * pieces + p
                    part = pl.ds(p * depth_down, depth_down)
                    loads_down[s, u, p] = store(
                        r.w_down.at[part, columns_of(dests[s] * t + shifted(tp, u, t))],
                        r.down.at[slot],
                        r.load_down.at[slot],
                    )

    affines = []

    def send_affine():
        for copy in small[1:]:
            copy.wait()
        r.affine[me, 0:1] = r.gain_one[...]
        r.affine[me, 1:2] = r.bias_one[...]
        for o, u in offsets:
            affines.append(
                send(
                    r.affine.at[me],
                    r.affine.at[me],
                    r.affine_send.at[o, u],
                    r.affine_recv.at[o, u],
                    at(o, u),
                )
            )
        pending.extend(affines)

    def pair_sum():
        parts = []
        for u in range(1, t):
            parts.append(
                send(
                    r.mixed.at[u],
                    r.part_got.at[u - 1],
                    r.part_send.at[u],
                    r.part_recv.at[u],
                    at(0, u),
                )
            )
        pending.extend(parts)
        own_tokens = r.tokens[:, columns_of(tp)].astype(jnp.float32)
        first = residual_scale * own_tokens + r.mixed[0]
        for u in range(1, t):
            parts[u - 1].wait_recv()
            first = first + r.part_got[u - 1]
        r.mixed[0] = first
        r.firsts[me] = first.astype(jnp.bfloat16)

    def hand_over(index, o, u, where):
        return pltpu.make_async_remote_copy(
            src_ref=r.firsts.at[index],
            dst_ref=r.firsts.at[index],
            send_sem=r.first_send.at[o, u],
            recv_sem=r.first_recv.at[o, u],
            device_id=where,
            device_id_type=MESH,
        )

    def tell_first():
        first = r.mixed[0]
        total = jnp.sum(first, axis=1, keepdims=True)
        away = first - total / columns
        r.tallies[0, 0:2] = jnp.concatenate(
            [to_lanes(total), to_lanes(jnp.sum(away * away, axis=1, keepdims=True))], axis=0
        )
        for i, (o, u) in enumerate(offsets):
            counts.append(
                send(
                    r.tallies.at[0],
                    r.tallies.at[i + 1],
                    r.tally_send.at[i],
                    r.tally_recv.at[i],
                    at(o, u),
                )
            )
        pending.extend(counts)

    counts = []
    def straight(o):
        return (kv != 0 if o == 3 else kv != 3) if relay and o != 2 else None

    def send_firsts():
        for u in range(1, t):
            copy = hand_over(me, 0, u, at(0, u))
            copy.start()
            pending.append(copy)
        for o in sorted(range(1, n), key=lambda o: -min(o, n - o)):
            copy = hand_over(me, o, 0, at(o, 0))
            guarded(straight(o), copy.start)

    def forward_first():
        return pltpu.make_async_remote_copy(
            src_ref=r.firsts.at[block(2, 0)],
            dst_ref=r.firsts.at[block(2, 0)],
            send_sem=r.forward_send,
            recv_sem=r.first_recv.at[2 * kv - 1, 0],
            device_id={"kv": buddy, "tp": tp},
            device_id_type=MESH,
        )

    def finish_firsts():
        for o in range(1, n):
            guarded(straight(o), hand_over(me, o, 0, at(o, 0)).wait_send)
        if relay:
            pl.when(is_relay)(lambda: forward_first().wait_send())

    def first_stats():
        for copy in affines:
            copy.wait_recv()
        for copy in counts:
            copy.wait_recv()
        tallies = [r.tallies[i, 0:2] for i in range(group)]
        center = sum(tally[0:1] for tally in tallies) / width
        spread = jnp.zeros_like(center)
        for tally in tallies:
            away = tally[0:1] / columns - center
            spread = spread + tally[1:2] + columns * (away * away)
        scale = lax.rsqrt(spread / width + epsilon)
        r.center[...] = jnp.broadcast_to(to_sublanes(center), r.center.shape)
        r.scale[...] = jnp.broadcast_to(to_sublanes(scale), r.scale.shape)

    def wait_first(o, u):
        hand_over(block(n - o, 0), o, u, at(0, u)).wait_recv()
        if u == 0:
            for v in range(1, t):
                copy = hand_over(block(n - o, 0), o, v, at(0, v))
                copy.start()
                pending.append(copy)

    def forward():
        if relay:
            pl.when(is_relay)(lambda: forward_first().start())

    def go_up(o, u, first_one):
        index = block(n - o, t - u)
        pair = r.affine[index]
        center, scale = r.center[:, 0:1], r.scale[:, 0:1]
        away = r.firsts[index].astype(jnp.float32) - center
        normed = (away * scale * pair[0:1] + pair[1:2]).astype(jnp.bfloat16)
        if first_one:
            r.own_normed[...] = normed
        for c in range(up_chunks):
            here = slice(c * up_width, (c + 1) * up_width)
            if first_one:
                loads_up[c].wait()
            product = jnp.dot(
                normed, r.up_buf[c, columns_of(index)], preferred_element_type=jnp.float32
            )
            r.upper[:, here] = product if first_one else r.upper[:, here] + product

    def square():
        upper = jnp.maximum(r.upper[...], 0.0)
        r.hidden[...] = (upper * upper).astype(jnp.bfloat16)

    near = {}

    def go_down(s, u):
        product = jnp.zeros((count, columns), jnp.float32)
        for p in range(pieces):
            loads_down[s, u, p].wait()
            product = product + jnp.dot(
                r.hidden[:, p * depth_down : (p + 1) * depth_down],
                r.down[(s * t + u) * pieces + p],
                preferred_element_type=jnp.float32,
            )
        if u:
            r.near_sent[s, u - 1] = product.astype(jnp.bfloat16)
            near[s, u] = send(
                r.near_sent.at[s, u - 1],
                r.near_got.at[s, u - 1],
                r.near_send.at[s, u - 1],
                r.near_recv.at[s, u - 1],
                at(0, u),
            )
        else:
            r.kept[s] = product

    def near_sum(s):
        value = r.kept[s]
        for u in range(1, t):
            near[s, u].wait_recv()
            value = value + r.near_got[s, u - 1].astype(jnp.float32)
        return value

    def far_copy(s, where):
        return pltpu.make_async_remote_copy(
            src_ref=r.far_sent.at[s],
            dst_ref=r.far_got.at[kv],
            send_sem=r.far_send.at[s],
            recv_sem=r.far_recv.at[kv],
            device_id={"kv": where, "tp": tp},
            device_id_type=MESH,
        )

    def far_relay():
        return pltpu.make_async_remote_copy(
            src_ref=r.far_sent.at[0],
            dst_ref=r.far_relay,
            send_sem=r.far_send.at[0],
            recv_sem=r.far_relay_recv,
            device_id={"kv": buddy, "tp": tp},
            device_id_type=MESH,
        )

    def far_out(s):
        value = near_sum(s)
        if relay and s == 0:
            r.far_sent[s] = value.astype(jnp.bfloat16)
            pl.when(is_end)(lambda: far_relay().start())
            pl.when(is_relay)(lambda: far_copy(s, dests[s]).start())
        elif relay and s == 2:
            r.kept[s] = value

            @pl.when(is_relay)
            def _():
                far_relay().wait_recv()
                r.kept[s] = r.kept[s] + r.far_relay[...].astype(jnp.float32)

            r.far_sent[s] = r.kept[s].astype(jnp.bfloat16)
            far_copy(s, dests[s]).start()
        else:
            r.far_sent[s] = value.astype(jnp.bfloat16)
            far_copy(s, dests[s]).start()

    def far_arrival(o):
        sender = shifted(kv, o, n)
        return pltpu.make_async_remote_copy(
            src_ref=r.far_sent.at[0],
            dst_ref=r.far_got.at[sender],
            send_sem=r.far_send.at[0],
            recv_sem=r.far_recv.at[sender],
            device_id={"kv": sender, "tp": tp},
            device_id_type=MESH,
        )

    def second_sum():
        second = residual_scale * r.own_normed[...].astype(jnp.float32) + near_sum(n - 1)
        for o in range(1, n):
            guarded(straight(o), far_arrival(o).wait_recv)
            second = second + r.far_got[shifted(kv, o, n)].astype(jnp.float32)
        r.kept[0] = second
        pending.extend(near.values())

    def second_norm():
        second = r.kept[0]
        sums = jnp.concatenate(
            [
                to_lanes(jnp.sum(second, axis=1, keepdims=True)),
                to_lanes(jnp.sum(second * second, axis=1, keepdims=True)),
            ],
            axis=0,
        )
        r.stats[0, 0:2] = sums
        tallies = []
        for i, (o, u) in enumerate(offsets):
            tallies.append(
                send(
                    r.stats.at[0],
                    r.stats.at[i + 1],
                    r.stats_send.at[i],
                    r.stats_recv.at[i],
                    at(o, u),
                )
            )
        pending.extend(tallies)
        for i, copy in enumerate(tallies):
            copy.wait_recv()
            sums = sums + r.stats[i + 1, 0:2]
        center_two = to_sublanes(sums[0:1]) / width
        spread_two = to_sublanes(sums[1:2]) / width - center_two * center_two
        result = (second - center_two) * lax.rsqrt(spread_two + epsilon)
        r.out[...] = (result * r.gain_two[...] + r.bias_two[...]).astype(jnp.bfloat16)

    def drain():
        for j in range(groups):
            finish_sends(j)
            finish_mixes(j)
        finish_firsts()
        for s in range(n - 1):
            far_copy(s, dests[s]).wait_send()
        for copy in pending:
            copy.wait_send()

    load_small([(r.tokens_in, r.tokens)])
    load_weights(0)
    greet_all()
    for j in range(1, groups):
        load_weights(j)
    load_small(vectors)
    wait_tokens()
    for j in range(groups):
        project(j)
        if j == 0:
            wait_barrier()
        send_far(j)
        send_near(j, is_relay if relay else None)
        if relay and j:
            send_near(j - 1, is_end)
        load_state(j)
    if relay:
        send_near(groups - 1, is_end)
    load_rest()
    for j in range(lead):
        pass_relay(j)
    send_affine()
    fill()
    for j in range(groups):
        wait_sums(j)
        prepare(j)
        update(j)
        gated_out(j)
        if j + lead < groups:
            pass_relay(j + lead)
    for j in range(groups):
        forward_mixes(j)
    for j in range(groups):
        wait_mixes(j)
        project_out(j)
    pair_sum()
    tell_first()
    send_firsts()
    wait_first(arrivals[0], 0)
    forward()
    first_stats()
    go_up(0, 0, True)
    for u in range(1, t):
        wait_first(0, u)
        go_up(0, u, False)
    for i in range(n - 1):
        if i:
            wait_first(arrivals[i], 0)
        go_up(arrivals[i], 0, False)
        if i:
            for u in range(1, t):
                wait_first(arrivals[i - 1], u)
                go_up(arrivals[i - 1], u, False)
    for u in range(1, t):
        wait_first(arrivals[-1], u)
        go_up(arrivals[-1], u, False)
    square()
    for s in range(n):
        for u in range(1, t):
            go_down(s, u)
        if s:
            far_out(s - 1)
        go_down(s, 0)
    second_sum()
    second_norm()
    drain()


def layer(n, t, tokens, state, weights, bound, gain, w_out, w_up, w_down, affine):
    count, depth = tokens.shape
    rows = count // n
    width = weights[0].shape[1]
    kinds = len(weights)
    size = state.shape[3]
    lanes = 2 * size
    wide = min(width, 8 * size)
    groups = width // wide
    heads = wide // size
    columns = affine[0].shape[1]
    model, units = w_up.shape
    group = n * t
    up_width = min(units, 512)
    dma = pltpu.SemaphoreType.DMA
    vmem = pltpu.VMEM
    few, many = jnp.bfloat16, jnp.float32
    shares = columns == wide and units % depth == 0 and group * (units // depth) == groups * kinds
    pieces = units // depth if shares else 1
    inputs = {
        "tokens_in": tokens,
        "state": state,
        "w_query": weights[0],
        "w_forget": weights[1],
        "w_input": weights[2],
        "w_gate": weights[3],
        "bound_in": bound,
        "gain_in": gain,
        "w_out": w_out,
        "w_up": w_up,
        "w_down": w_down,
        "gain_one_in": affine[0],
        "bias_one_in": affine[1],
        "gain_two_in": affine[2],
        "bias_two_in": affine[3],
    }
    scratch = {
        "tokens": vmem(tokens.shape, few),
        "bound": vmem(bound.shape, many),
        "gain": vmem(gain.shape, many),
        "gain_one": vmem((1, columns), many),
        "bias_one": vmem((1, columns), many),
        "gain_two": vmem((1, columns), many),
        "bias_two": vmem((1, columns), many),
        "pool": vmem((groups * kinds, depth, wide), few),
        "whole": vmem((groups, kinds, n, rows, wide), many),
        "sent": vmem((groups, n, kinds, rows, wide), few),
        "got": vmem((groups, 2 if n == 4 else n - 1, kinds, rows, wide), few),
        "relay_got": vmem((groups, 2, kinds, rows, wide), few),
        "relay_sent": vmem((groups, 2, kinds, rows, wide), few),
        "pick": vmem((4 * rows, rows * 2 * lanes), few),
        "factors": vmem((heads, size, 4 * rows), few),
        "value": vmem((heads, rows, lanes), many),
        "gate": vmem((rows, wide), many),
        "spread": vmem((2, size, rows * 2 * lanes), many),
        "read": vmem((heads, rows, size), many),
        "gathered": vmem((groups, n, rows, wide), few),
        "out_buf": vmem((t, width, columns), few),
        "mixed": vmem((t, count, columns), many),
        "up_buf": vmem((units // up_width, model, up_width), few),
        "part_got": vmem((t - 1, count, columns), many),
        "affine": vmem((group, 2, columns), many),
        "firsts": vmem((group, count, columns), few),
        "tallies": vmem((group, 8, count), many),
        "center": vmem((count, 128), many),
        "scale": vmem((count, 128), many),
        "upper": vmem((count, units), many),
        "own_normed": vmem((count, columns), few),
        "hidden": vmem((count, units), few),
        "near_sent": vmem((n, t - 1, count, columns), few),
        "near_got": vmem((n, t - 1, count, columns), few),
        "kept": vmem((n, count, columns), many),
        "far_sent": vmem((n, count, columns), few),
        "far_got": vmem((n, count, columns), few),
        "far_relay": vmem((count, columns), few),
        "stats": vmem((group, 8, count), many),
        "small_sem": dma((7,)),
        "load_project": dma((groups * kinds,)),
        "load_state": dma((groups,)),
        "load_out": dma((t,)),
        "load_up": dma((units // up_width,)),
        "load_down": dma((group * pieces,)),
        "sum_send": dma((groups, n - 1)),
        "sum_recv": dma((groups, n - 1)),
        "relay_send": dma((groups, 2)),
        "relay_recv": dma((groups, 2)),
        "forward_send": dma,
        "far_relay_recv": dma,
        "mix_send": dma((groups, n)),
        "mix_recv": dma((groups, n)),
        "mix_forward": dma((groups, 2)),
        "tally_send": dma((group,)),
        "tally_recv": dma((group,)),
        "part_send": dma((t,)),
        "part_recv": dma((t,)),
        "affine_send": dma((n, t)),
        "affine_recv": dma((n, t)),
        "first_send": dma((n, t)),
        "first_recv": dma((n, t)),
        "near_send": dma((n, t)),
        "near_recv": dma((n, t)),
        "far_send": dma((n,)),
        "far_recv": dma((n,)),
        "stats_send": dma((group,)),
        "stats_recv": dma((group,)),
    }
    if not shares:
        scratch["down"] = vmem((group, units, columns), few)

    def kernel(*refs):
        names = [*inputs, "out", "new_state", *scratch]
        if shares:
            names.append("down")
            refs = (*refs, refs[names.index("pool")])
        layer_kernel(n, t, size, names, *refs)

    return pl.pallas_call(
        kernel,
        out_shape=(vmem((count, columns), few), vmem(state.shape, many)),
        in_specs=[pl.BlockSpec(memory_space=pl.ANY)] * len(inputs),
        out_specs=(pl.BlockSpec(memory_space=pltpu.VMEM),) * 2,
        scratch_shapes=list(scratch.values()),
        compiler_params=pltpu.CompilerParams(
            collective_id=0, has_side_effects=True, vmem_limit_bytes=LAYER_BYTES
        ),
        name="layer",
    )(*inputs.values())


def write_kernel(result, new_state, result_out, state_out, sem):
    pieces = sem.shape[0] - 1
    heads = new_state.shape[1] // pieces
    copies = [store(result, result_out, sem.at[pieces])]
    for i in range(pieces):
        part = pl.ds(i * heads, heads)
        copies.append(store(new_state.at[:, part], state_out.at[:, part], sem.at[i]))
    for copy in copies:
        copy.wait()


def write_out(result, new_state):
    return pl.pallas_call(
        write_kernel,
        out_shape=(
            jax.ShapeDtypeStruct(result.shape, result.dtype),
            jax.ShapeDtypeStruct(new_state.shape, new_state.dtype),
        ),
        in_specs=[pl.BlockSpec(memory_space=pltpu.VMEM)] * 2,
        out_specs=(pl.BlockSpec(memory_space=pl.ANY),) * 2,
        scratch_shapes=[pltpu.SemaphoreType.DMA((9,))],
        compiler_params=pltpu.CompilerParams(vmem_limit_bytes=WRITE_BYTES),
        name="write",
    )(result, new_state)


def per_device(
    tokens,
    state,
    w_query,
    w_forget,
    w_input,
    w_gate,
    lower_bound,
    head_gain,
    w_out,
    gain_one,
    bias_one,
    w_up,
    w_down,
    gain_two,
    bias_two,
):
    n, t = lax.axis_size("kv"), lax.axis_size("tp")
    result, new_state = layer(
        n,
        t,
        tokens,
        state,
        (w_query, w_forget, w_input, w_gate),
        lower_bound[None, :],
        jnp.tile(head_gain, 2)[None, :],
        w_out,
        w_up,
        w_down,
        [vector[None, :] for vector in (gain_one, bias_one, gain_two, bias_two)],
    )
    return write_out(result, new_state)


def solution(mesh):
    placed = (
        P("dp", "kv"),
        P(("dp", "kv"), "tp", None, None),
        P("kv", "tp"),
        P("kv", "tp"),
        P("kv", "tp"),
        P("kv", "tp"),
        P("tp"),
        P(),
        P("tp", "kv"),
        P(("kv", "tp")),
        P(("kv", "tp")),
        P(None, ("kv", "tp")),
        P(("kv", "tp"), None),
        P(("kv", "tp")),
        P(("kv", "tp")),
    )
    return jax.shard_map(
        per_device,
        mesh=mesh,
        in_specs=placed,
        out_specs=(P("dp", ("kv", "tp")), P(("dp", "kv"), "tp", None, None)),
        check_vma=False,
    )
```

time: 78.1 us -> 67 us (0.86)
  Pallas kernels: 76.1 us -> 64.9 us
    pallas_call x1, Pallas kernels: 70.1 us -> 59 us  [layer(): pl.pallas_call(kernel, out_shape=(vmem((count, columns), few), vmem(state...]
where the time goes in v2:
time: 67 us; the launch traced here: 66.8 us
  Pallas kernels  64.9 us (97%)
  local copies, waits for them, and re-layouts  1.25 us (2%)
    pallas_call x1, Pallas kernels, layer(): pl.pallas_call(kernel, out_shape=(vmem((count, columns), few), vmem(state...  59 us
    pallas_call x1, Pallas kernels, write_out(): pl.pallas_call(write_kernel, out_shape=(jax.ShapeDtypeStruct(result.shape...  5.95 us

profile of v2, /device:TPU:0, one launch (start us, length us, event | category | flops | bytes accessed | tf_op | source)
XLA Modules:
  0.0 66.8 jit_solution(11159714903497889345)
XLA Ops:
  0.6 0.7 tile.2
  1.3 0.6 broadcast_in_dim_tile.3.refs_7_
  1.9 59.0 %layer.1 = (bf16[64,512]{1,0:T(8,128)(2,1)S(1)}, f32[16,32,64,64]{3,2,1,0:T(8,128)S(1)}) custom-call(bf16[64,1024]{1,0:T(8,128)(2,1)} %refs_0_.1, f32[16,32,64,64]{3,2,1,0:T(8,128)} %refs_1_.1, bf16[1024,2048]{1,0:T(8,128)(2,1)} %refs_2_.1, bf16[1024,2048]{1,0:T(8,128)(2,1)} %refs_3_.1, bf16[1024,2048]{1,0:T(8,128)(2,1)} %refs_4_.1, ...), custom_call_target="tpu_custom_call" | custom-call | tf_op jit(solution)/shard_map/layer/pallas_call | solution.py:872
  60.9 6.0 %write.1 = (bf16[64,512]{1,0:T(8,128)(2,1)}, f32[16,32,64,64]{3,2,1,0:T(8,128)}) custom-call(bf16[64,512]{1,0:T(8,128)(2,1)S(1)} %get-tuple-element.4.result, f32[16,32,64,64]{3,2,1,0:T(8,128)S(1)} %get-tuple-element.5.new_state), custom_call_target="tpu_custom_call" | custom-call | tf_op jit(solution)/shard_map/write/pallas_call | solution.py:897

commit v3 on v2

--- a/solution.py
+++ b/solution.py
@@ -14,6 +14,9 @@
 MESH = pl.DeviceIdType.MESH
 LAYER_BYTES = 47 * 1024 * 1024
 WRITE_BYTES = 1024 * 1024
+GROUP_HEADS = 4
+LAG = 3
+LEAD = 5
 
 
 def shifted(index, by, count):
@@ -121,12 +124,15 @@
     weights = (r.w_query, r.w_forget, r.w_input, r.w_gate)
     loads = {}
 
-    def load_weights(j):
+    span = r.pool.shape[2]
+    parts = span // wide
+
+    def load_weights(c):
         for w in range(kinds):
-            loads[j, w] = store(
-                weights[w].at[:, pl.ds(j * wide, wide)],
-                r.pool.at[j * kinds + w],
-                r.load_project.at[j * kinds + w],
+            loads[c, w] = store(
+                weights[w].at[:, pl.ds(c * span, span)],
+                r.pool.at[c * kinds + w],
+                r.load_project.at[c * kinds + w],
             )
 
     def wait_tokens():
@@ -170,7 +176,8 @@
     ]
     is_end = (kv == 0) | (kv == n - 1)
     is_relay = (kv != 0) & (kv != n - 1)
-    lead = min(2, groups)
+    lag = LAG
+    lead = min(LEAD, groups)
 
     def to_relay(j, i):
         return pltpu.make_async_remote_copy(
@@ -193,14 +200,16 @@
             device_id_type=MESH,
         )
 
-    def project(j):
+    def project(c):
         for w in range(kinds):
-            loads[j, w].wait()
+            loads[c, w].wait()
             value = jnp.dot(
-                r.tokens[...], r.pool[j * kinds + w], preferred_element_type=jnp.float32
-            ).reshape(n, rows, wide)
-            r.whole[j, w] = value
-            r.sent[j, :, w] = value.astype(jnp.bfloat16)
+                r.tokens[...], r.pool[c * kinds + w], preferred_element_type=jnp.float32
+            ).reshape(n, rows, span)
+            for p in range(parts):
+                here = value[:, :, p * wide : (p + 1) * wide]
+                r.whole[c * parts + p, w] = here
+                r.sent[c * parts + p, :, w] = here.astype(jnp.bfloat16)
 
     def send_far(j):
         if relay:
@@ -300,10 +309,11 @@
             whole = r.read[h]
             return whole * lax.rsqrt(jnp.mean(whole * whole, axis=1, keepdims=True) + epsilon)
 
+        gain = jnp.concatenate([r.gain[...]] * 2, axis=1)
         for p in range(heads // 2):
             here = slice(p * lanes, (p + 1) * lanes)
             pair = jnp.concatenate([normalized(2 * p), normalized(2 * p + 1)], axis=1)
-            gated = pair * r.gain[...] * r.gate[:, here]
+            gated = pair * gain * r.gate[:, here]
             r.gathered[j, kv, :, here] = gated.astype(jnp.bfloat16)
         for o in range(1, n):
             guarded(sends_mix(j, o), mix_copy(j, o).start)
@@ -688,21 +698,23 @@
     load_small([(r.tokens_in, r.tokens)])
     load_weights(0)
     greet_all()
-    for j in range(1, groups):
-        load_weights(j)
+    for c in range(1, groups // parts):
+        load_weights(c)
     load_small(vectors)
     wait_tokens()
-    for j in range(groups):
-        project(j)
-        if j == 0:
+    for c in range(groups // parts):
+        project(c)
+        if c == 0:
             wait_barrier()
-        send_far(j)
-        send_near(j, is_relay if relay else None)
-        if relay and j:
-            send_near(j - 1, is_end)
-        load_state(j)
+        for j in range(c * parts, (c + 1) * parts):
+            send_far(j)
+            send_near(j, is_relay if relay else None)
+            if relay and j >= lag:
+                send_near(j - lag, is_end)
+            load_state(j)
     if relay:
-        send_near(groups - 1, is_end)
+        for j in range(max(groups - lag, 0), groups):
+            send_near(j, is_end)
     load_rest()
     for j in range(lead):
         pass_relay(j)
@@ -723,10 +735,10 @@
     pair_sum()
     tell_first()
     send_firsts()
+    first_stats()
+    go_up(0, 0, True)
     wait_first(arrivals[0], 0)
     forward()
-    first_stats()
-    go_up(0, 0, True)
     for u in range(1, t):
         wait_first(0, u)
         go_up(0, u, False)
@@ -760,7 +772,8 @@
     kinds = len(weights)
     size = state.shape[3]
     lanes = 2 * size
-    wide = min(width, 8 * size)
+    wide = min(width, GROUP_HEADS * size)
+    span = min(width, 8 * size)
     groups = width // wide
     heads = wide // size
     columns = affine[0].shape[1]
@@ -770,7 +783,8 @@
     dma = pltpu.SemaphoreType.DMA
     vmem = pltpu.VMEM
     few, many = jnp.bfloat16, jnp.float32
-    shares = columns == wide and units % depth == 0 and group * (units // depth) == groups * kinds
+    chunks = width // span * kinds
+    shares = columns == span and units % depth == 0 and group * (units // depth) == chunks
     pieces = units // depth if shares else 1
     inputs = {
         "tokens_in": tokens,
@@ -797,7 +811,7 @@
         "bias_one": vmem((1, columns), many),
         "gain_two": vmem((1, columns), many),
         "bias_two": vmem((1, columns), many),
-        "pool": vmem((groups * kinds, depth, wide), few),
+        "pool": vmem((chunks, depth, span), few),
         "whole": vmem((groups, kinds, n, rows, wide), many),
         "sent": vmem((groups, n, kinds, rows, wide), few),
         "got": vmem((groups, 2 if n == 4 else n - 1, kinds, rows, wide), few),
@@ -830,7 +844,7 @@
         "far_relay": vmem((count, columns), few),
         "stats": vmem((group, 8, count), many),
         "small_sem": dma((7,)),
-        "load_project": dma((groups * kinds,)),
+        "load_project": dma((chunks,)),
         "load_state": dma((groups,)),
         "load_out": dma((t,)),
         "load_up": dma((units // up_width,)),
@@ -933,7 +947,7 @@
         state,
         (w_query, w_forget, w_input, w_gate),
         lower_bound[None, :],
-        jnp.tile(head_gain, 2)[None, :],
+        head_gain[None, :],
         w_out,
         w_up,
         w_down,

time: 67 us -> 65.3 us (0.975)
  local copies, waits for them, and re-layouts: 1.25 us -> 0 us
    another operation x2 -> x0, local copies, waits for them, and re-layouts: 1.25 us -> none  [per_device(): jnp.tile(head_gain, 2)[None, :]]
where the time goes in v3:
time: 65.3 us; the launch traced here: 65.1 us
  Pallas kernels  64.5 us (99%)
    pallas_call x1, Pallas kernels, layer(): pl.pallas_call(kernel, out_shape=(vmem((count, columns), few), vmem(state...  58.5 us
    pallas_call x1, Pallas kernels, write_out(): pl.pallas_call(write_kernel, out_shape=(jax.ShapeDtypeStruct(result.shape...  5.95 us

profile of v3, /device:TPU:0, one launch (start us, length us, event | category | flops | bytes accessed | tf_op | source)
XLA Modules:
  0.0 65.1 jit_solution(167137773526798070)
XLA Ops:
  0.6 58.5 %layer.1 = (bf16[64,512]{1,0:T(8,128)(2,1)S(1)}, f32[16,32,64,64]{3,2,1,0:T(8,128)S(1)}) custom-call(bf16[64,1024]{1,0:T(8,128)(2,1)} %refs_0_.1, f32[16,32,64,64]{3,2,1,0:T(8,128)} %refs_1_.1, bf16[1024,2048]{1,0:T(8,128)(2,1)} %refs_2_.1, bf16[1024,2048]{1,0:T(8,128)(2,1)} %refs_3_.1, bf16[1024,2048]{1,0:T(8,128)(2,1)} %refs_4_.1, ...), custom_call_target="tpu_custom_call" | custom-call | tf_op jit(solution)/shard_map/layer/pallas_call | solution.py:886
  59.1 6.0 %write.1 = (bf16[64,512]{1,0:T(8,128)(2,1)}, f32[16,32,64,64]{3,2,1,0:T(8,128)}) custom-call(bf16[64,512]{1,0:T(8,128)(2,1)S(1)} %get-tuple-element.4.result, f32[16,32,64,64]{3,2,1,0:T(8,128)S(1)} %get-tuple-element.5.new_state), custom_call_target="tpu_custom_call" | custom-call | tf_op jit(solution)/shard_map/write/pallas_call | solution.py:911

commit v4 on v3

--- a/solution.py
+++ b/solution.py
@@ -126,6 +126,7 @@
 
     span = r.pool.shape[2]
     parts = span // wide
+    extra = r.scaled.shape[1] - count
 
     def load_weights(c):
         for w in range(kinds):
@@ -329,7 +330,7 @@
         )
 
     def hops(j):
-        return relay and j < groups - 1
+        return relay and j < groups - 2
 
     def sends_mix(j, o):
         return (kv != 3 if o == 1 else kv != 0 if o == 3 else is_relay) if hops(j) else None
@@ -519,8 +520,6 @@
             pl.when(is_relay)(lambda: forward_first().wait_send())
 
     def first_stats():
-        for copy in affines:
-            copy.wait_recv()
         for copy in counts:
             copy.wait_recv()
         tallies = [r.tallies[i, 0:2] for i in range(group)]
@@ -545,26 +544,41 @@
         if relay:
             pl.when(is_relay)(lambda: forward_first().start())
 
+    def stack_affine():
+        for copy in affines:
+            copy.wait_recv()
+        for g in range(group):
+            pair = r.affine[g]
+            high = pair.astype(jnp.bfloat16).astype(jnp.float32)
+            lines = [high, pair - high, jnp.zeros((extra - 4, columns), jnp.float32)]
+            r.scaled[g, count:] = jnp.concatenate(lines, axis=0).astype(jnp.bfloat16)
+
     def go_up(o, u, first_one):
         index = block(n - o, t - u)
-        pair = r.affine[index]
-        center, scale = r.center[:, 0:1], r.scale[:, 0:1]
-        away = r.firsts[index].astype(jnp.float32) - center
-        normed = (away * scale * pair[0:1] + pair[1:2]).astype(jnp.bfloat16)
-        if first_one:
-            r.own_normed[...] = normed
+        gain = r.affine[index, 0:1]
+        r.scaled[index, :count] = (r.firsts[index].astype(jnp.float32) * gain).astype(jnp.bfloat16)
         for c in range(up_chunks):
             here = slice(c * up_width, (c + 1) * up_width)
             if first_one:
                 loads_up[c].wait()
             product = jnp.dot(
-                normed, r.up_buf[c, columns_of(index)], preferred_element_type=jnp.float32
+                r.scaled[index],
+                r.up_buf[c, columns_of(index)],
+                preferred_element_type=jnp.float32,
             )
             r.upper[:, here] = product if first_one else r.upper[:, here] + product
 
     def square():
-        upper = jnp.maximum(r.upper[...], 0.0)
-        r.hidden[...] = (upper * upper).astype(jnp.bfloat16)
+        center, scale = r.center[:, 0:1], r.scale[:, 0:1]
+        for c in range(up_chunks):
+            here = slice(c * up_width, (c + 1) * up_width)
+            tail = r.upper[count : count + 4, here]
+            gain, bias = tail[0:1] + tail[2:3], tail[1:2] + tail[3:4]
+            upper = jnp.maximum((r.upper[:count, here] - center * gain) * scale + bias, 0.0)
+            r.hidden[:, here] = (upper * upper).astype(jnp.bfloat16)
+        pair = r.affine[me]
+        away = r.firsts[me].astype(jnp.float32) - center
+        r.own_normed[...] = (away * scale * pair[0:1] + pair[1:2]).astype(jnp.bfloat16)
 
     near = {}
 
@@ -729,27 +743,27 @@
             pass_relay(j + lead)
     for j in range(groups):
         forward_mixes(j)
+    stack_affine()
     for j in range(groups):
         wait_mixes(j)
         project_out(j)
     pair_sum()
+    send_firsts()
     tell_first()
-    send_firsts()
-    first_stats()
     go_up(0, 0, True)
-    wait_first(arrivals[0], 0)
-    forward()
     for u in range(1, t):
         wait_first(0, u)
         go_up(0, u, False)
-    for i in range(n - 1):
-        if i:
-            wait_first(arrivals[i], 0)
+    wait_first(arrivals[0], 0)
+    forward()
+    go_up(arrivals[0], 0, False)
+    for i in range(1, n - 1):
+        wait_first(arrivals[i], 0)
         go_up(arrivals[i], 0, False)
-        if i:
-            for u in range(1, t):
-                wait_first(arrivals[i - 1], u)
-                go_up(arrivals[i - 1], u, False)
+        for u in range(1, t):
+            wait_first(arrivals[i - 1], u)
+            go_up(arrivals[i - 1], u, False)
+    first_stats()
     for u in range(1, t):
         wait_first(arrivals[-1], u)
         go_up(arrivals[-1], u, False)
@@ -833,7 +847,8 @@
         "tallies": vmem((group, 8, count), many),
         "center": vmem((count, 128), many),
         "scale": vmem((count, 128), many),
-        "upper": vmem((count, units), many),
+        "scaled": vmem((group, count + 16, columns), few),
+        "upper": vmem((count + 16, units), many),
         "own_normed": vmem((count, columns), few),
         "hidden": vmem((count, units), few),
         "near_sent": vmem((n, t - 1, count, columns), few),

time: 65.3 us -> 64.1 us (0.982)
  Pallas kernels: 64.5 us -> 63.3 us
    pallas_call x1, Pallas kernels: 58.5 us -> 57.4 us  [layer(): pl.pallas_call(kernel, out_shape=(vmem((count, columns), few), vmem(state...]
where the time goes in v4:
time: 64.1 us; the launch traced here: 64 us
  Pallas kernels  63.3 us (99%)
    pallas_call x1, Pallas kernels, layer(): pl.pallas_call(kernel, out_shape=(vmem((count, columns), few), vmem(state...  57.4 us
    pallas_call x1, Pallas kernels, write_out(): pl.pallas_call(write_kernel, out_shape=(jax.ShapeDtypeStruct(result.shape...  5.95 us

profile of v4, /device:TPU:0, one launch (start us, length us, event | category | flops | bytes accessed | tf_op | source)
XLA Modules:
  0.0 64.0 jit_solution(15007674082390831459)
XLA Ops:
  0.6 57.4 %layer.1 = (bf16[64,512]{1,0:T(8,128)(2,1)S(1)}, f32[16,32,64,64]{3,2,1,0:T(8,128)S(1)}) custom-call(bf16[64,1024]{1,0:T(8,128)(2,1)} %refs_0_.1, f32[16,32,64,64]{3,2,1,0:T(8,128)} %refs_1_.1, bf16[1024,2048]{1,0:T(8,128)(2,1)} %refs_2_.1, bf16[1024,2048]{1,0:T(8,128)(2,1)} %refs_3_.1, bf16[1024,2048]{1,0:T(8,128)(2,1)} %refs_4_.1, ...), custom_call_target="tpu_custom_call" | custom-call | tf_op jit(solution)/shard_map/layer/pallas_call | solution.py:901
  58.0 6.0 %write.1 = (bf16[64,512]{1,0:T(8,128)(2,1)}, f32[16,32,64,64]{3,2,1,0:T(8,128)}) custom-call(bf16[64,512]{1,0:T(8,128)(2,1)S(1)} %get-tuple-element.4.result, f32[16,32,64,64]{3,2,1,0:T(8,128)S(1)} %get-tuple-element.5.new_state), custom_call_target="tpu_custom_call" | custom-call | tf_op jit(solution)/shard_map/write/pallas_call | solution.py:926
